TPU v7x, 1024 devices: a whole 4x8x16 slice. The times are simulated.
1024 devices in a mesh: sp: 128 (over z, y), tp: 8 (over x, core).
Axes of the slice: x: 4, y: 8, z: 16, core: 2. Of those that a mesh axis runs over, the one named last changes fastest.
Arguments:
- tokens: bfloat16 [4, 16384, 2048], P(None, 'sp'), may hold values from -6 to 6
- next_tokens: bfloat16 [4, 2048], replicated, may hold values from -6 to 6
- w_query: bfloat16 [2048, 2048], P(None, 'tp'), may hold values from -0.125 to 0.125
- w_key: bfloat16 [2048, 2048], P(None, 'tp'), may hold values from -0.125 to 0.125
- w_value: bfloat16 [2048, 2048], P(None, 'tp'), may hold values from -0.125 to 0.125
- w_in_gate: bfloat16 [2048, 8], replicated, may hold values from -0.125 to 0.125
- w_forget_gate: bfloat16 [2048, 8], replicated, may hold values from -0.125 to 0.125
- forget_bias: float32 [8], replicated, may hold values from 3 to 14
- extra_decay: float32 [8, 4, 16384], P('tp', None, 'sp'), may hold values from -0.55006104 to 0
- w_out: bfloat16 [2048, 2048], P('tp'), may hold values from -0.125 to 0.125
Outputs:
- memory: bfloat16 [8, 1024, 256], P('tp', 'sp')
- normalizer: float32 [8, 1024], P('tp', 'sp')
- stabilizer: float32 [4, 8], P(None, 'tp')
- read: bfloat16 [4, 2048], replicated
All inputs are finite; a program needn't handle non-finite values.
Results may differ from a plain program's by a relative error of at most 0.024.
Values may be sent and summed in bfloat16 or wider, within the bound.
No kernel may reach another device: no remote copies, remote signals or barrier semaphores. Data moves between devices by JAX's collectives and lax.ppermute only.
A program may use at most 32 MiB of HBM per device.

v0:
```python
import functools

import jax
import jax.numpy as jnp
from jax import lax
from jax.sharding import Mesh
from jax.sharding import PartitionSpec as P

HD = 256
SP = ("sp_0", "sp_1")


def sent_together(arrays, axis, dim, along):
    ends, at = ([], 0)
    for a in arrays[:-1]:
        at += a.shape[along]
        ends.append(at)
    both = jnp.concatenate(arrays, axis=along)
    return tuple(jnp.split(lax.all_gather(both, axis, axis=dim, tiled=True), ends, axis=along))


def sum_by_axis(value, axes, dim):
    if not axes:
        return value
    nearer = lax.psum_scatter(value, axes[0], scatter_dimension=dim, tiled=True)
    return sum_by_axis(nearer, axes[1:], dim)


def by_axis(value, axes):
    return functools.reduce(lax.psum, axes, value)


def copy_for_each(value, axis):
    count = lax.axis_size(axis)
    return lax.all_to_all(
        jnp.broadcast_to(value[None], (count, *value.shape)), axis, 0, 0, tiled=True
    )


def of_everyone(value, axis):
    return copy_for_each(value, axis).astype(jnp.float32).sum(axis=0)


def per_device(
    tokens,
    next_tokens,
    w_query,
    w_key,
    w_value,
    w_in_gate,
    w_forget_gate,
    forget_bias,
    extra_decay,
    w_out,
):
    scale = HD ** (-0.5)
    seq_count = tokens.shape[0]
    span = tokens.shape[1]
    heads_here = w_key.shape[1] // HD
    sp_size = lax.axis_size(SP)
    sp_index = lax.axis_index(SP)
    head_start = lax.axis_index("tp") * heads_here
    gate_in = lax.dynamic_slice_in_dim(w_in_gate, head_start, heads_here, 1)
    gate_forget = lax.dynamic_slice_in_dim(w_forget_gate, head_start, heads_here, 1)
    bias_here = lax.dynamic_slice_in_dim(forget_bias, head_start, heads_here, 0)
    flat = tokens.reshape(seq_count * span, tokens.shape[2])
    keys = jnp.dot(flat, w_key, preferred_element_type=jnp.float32).astype(jnp.bfloat16)
    values = jnp.dot(flat, w_value, preferred_element_type=jnp.float32).astype(jnp.bfloat16)
    log_in = jnp.dot(flat, gate_in, preferred_element_type=jnp.float32).reshape(
        seq_count, span, heads_here
    )
    log_forget = jax.nn.log_sigmoid(
        jnp.dot(flat, gate_forget, preferred_element_type=jnp.float32) + bias_here
    ).reshape(seq_count, span, heads_here) + jnp.transpose(extra_decay, (1, 2, 0))
    prefix = jnp.cumsum(log_forget, axis=1)
    block_total = prefix[:, -1]
    local_score = block_total[:, None, :] - prefix + log_in
    block_peak = jnp.max(local_score, axis=1)
    totals, peaks = sent_together((block_total[None], block_peak[None]), SP, 0, 1)
    later = jnp.flip(jnp.cumsum(jnp.flip(totals, 0), axis=0), 0) - totals
    prompt_total = jnp.sum(totals, axis=0)
    stabilizer = jnp.maximum(prompt_total, jnp.max(later + peaks, axis=0))
    pick_block = (jnp.arange(sp_size) == sp_index).astype(jnp.float32)
    later_here = jnp.sum(pick_block[:, None, None] * later, axis=0)
    weight = jnp.exp(later_here[:, None, :] + local_score - stabilizer[:, None, :]) * scale
    key_heads = keys.reshape(seq_count, span, heads_here, HD)
    value_heads = values.reshape(seq_count, span, heads_here, HD)
    weighted = (key_heads.astype(jnp.float32) * weight[:, :, :, None]).astype(jnp.bfloat16)
    block_memory = jnp.einsum(
        "sthd,sthe->hsde", weighted, value_heads, preferred_element_type=jnp.float32
    )
    block_norm = jnp.transpose(jnp.sum(weighted.astype(jnp.float32), axis=1), (1, 0, 2))
    memory_term = block_memory.reshape(heads_here, seq_count * HD, HD)
    norm_term = block_norm.reshape(heads_here, seq_count * HD)
    memory_rows, norm_rows = (sum_by_axis(memory_term, SP, 1), sum_by_axis(norm_term, SP, 1))
    query = (
        jnp.dot(next_tokens, w_query, preferred_element_type=jnp.float32)
        .astype(jnp.bfloat16)
        .astype(jnp.float32)
        .reshape(seq_count, heads_here, HD)
    )
    new_key = (
        jnp.dot(next_tokens, w_key, preferred_element_type=jnp.float32)
        .astype(jnp.bfloat16)
        .astype(jnp.float32)
        .reshape(seq_count, heads_here, HD)
        * scale
    )
    new_value = (
        jnp.dot(next_tokens, w_value, preferred_element_type=jnp.float32)
        .astype(jnp.bfloat16)
        .astype(jnp.float32)
        .reshape(seq_count, heads_here, HD)
    )
    new_in = jnp.dot(next_tokens, gate_in, preferred_element_type=jnp.float32)
    new_forget = jax.nn.log_sigmoid(
        jnp.dot(next_tokens, gate_forget, preferred_element_type=jnp.float32) + bias_here
    )
    numer_slots = jnp.einsum("shd,hsde->she", query, block_memory, precision=lax.Precision.HIGHEST)
    denom_slots = jnp.einsum("shd,hsd->sh", query, block_norm, precision=lax.Precision.HIGHEST)
    query_state, query_norm = (by_axis(numer_slots, SP), by_axis(denom_slots, SP))
    top = jnp.maximum(new_forget + stabilizer, new_in)
    keep = jnp.exp(new_forget + stabilizer - top)
    take = jnp.exp(new_in - top)
    qk = jnp.sum(query * new_key, axis=-1)
    numer = keep[:, :, None] * query_state + (take * qk)[:, :, None] * new_value
    denom = keep * query_norm + take * qk
    head_out = (numer / jnp.maximum(jnp.abs(denom), 1.0)[:, :, None]).astype(jnp.bfloat16)
    partial_value = (
        jnp.dot(
            head_out.reshape(seq_count, heads_here * HD), w_out, preferred_element_type=jnp.float32
        )
        .astype(jnp.bfloat16)
        .astype(jnp.float32)
    )
    read = (
        of_everyone(partial_value.astype(jnp.bfloat16), "tp")
        .astype(jnp.float32)
        .astype(jnp.bfloat16)
    )
    return (memory_rows.astype(jnp.bfloat16), norm_rows, stabilizer, read)


def solution(mesh):
    torus = Mesh(mesh.devices.reshape(16, 8, mesh.shape["tp"]), ("sp_0", "sp_1", "tp"))
    placed = (
        P(None, SP, None),
        P(),
        P(None, "tp"),
        P(None, "tp"),
        P(None, "tp"),
        P(),
        P(),
        P(),
        P("tp", None, SP),
        P("tp", None),
    )
    return jax.shard_map(
        per_device,
        mesh=torus,
        in_specs=placed,
        out_specs=(P("tp", SP, None), P("tp", SP), P(None, "tp"), P()),
        check_vma=False,
    )
```

profile of v0, /device:TPU:1, one launch (start us, length us, event | category | flops | bytes accessed | tf_op | source)
XLA Modules:
  0.0 301.4 jit_solution(7201836543060438226)
XLA Ops:
  7.2 0.0 reduce-scatter.11.cloned.1.call-start
  7.3 1.4 dynamic_slice.10
  8.6 0.1 copy-done
  8.8 1.4 fusion.16
  10.2 0.7 fusion.24
  10.9 0.7 fusion.29
  11.5 0.2 copy.30
  11.7 0.3 reduce_window_sum.24
  12.0 0.1 slice_reduce_fusion
  12.1 0.1 reduce.12
  12.2 0.2 fusion.47
  12.4 0.1 pad_maximum_fusion
  12.5 73.7 %all_gather.3 = f32[128,8,1]{1,2,0:T(1,128)S(1)} all-gather(f32[1,8,1]{1,2,0:T(1,128)S(1)} %pad_maximum_fusion), channel_id=1, replica_groups=mesh['sp_0'=16,'sp_1'=8,'tp'=8] {'sp_0','sp_1'}, dimensions={0}, use_global_device_ids=true | all-gather | bytes 4128 | tf_op jit(solution)/shard_map/all_gather | solution.py:19
  86.2 0.2 fusion.50
  86.4 0.9 copy.48
  87.3 0.9 copy.47
  88.3 0.1 fusion.53
  88.4 1.9 fusion
  90.3 0.3 multiply_reduce_fusion
  90.7 0.1 exponential_multiply_fusion
  90.7 0.2 convert_reduce_fusion
  90.9 0.2 copy.51
  91.1 0.9 bitcast_bitcast_fusion
  92.0 0.0 reduce-scatter.11.cloned.1.call-update
  92.0 0.0 reduce-scatter.7.cloned.1.call-start
  92.1 1.9 convolution_convert_fusion.1
  94.0 0.2 copy.33
  94.2 1.3 fusion.14
  95.5 0.0 reduce-scatter.9.cloned.1.call-start
  95.6 1.7 fusion.18
  97.3 0.4 fusion.19
  97.7 21.3 %all-reduce.1 = (f32[4,1,256]{2,0,1:T(4,128)S(1)}, f32[4,1]{0,1:T(1,128)S(1)}) all-reduce(f32[4,1,256]{2,0,1:T(4,128)S(1)} %copy.37, f32[4,1]{0,1:T(1,128)S(1)} %bitcast.113), channel_id=1, replica_groups=mesh['sp_0'=16,'sp_1'=8,'tp'=8] {'sp_0'}, use_global_device_ids=true, to_apply=%region_11.12 | all-reduce | flops 1028 | bytes 8224 | tf_op jit(solution)/shard_map/psum | solution.py:30
  119.1 0.9 convolution_bitcast_fusion
  120.0 1.6 fusion.10
  121.5 46.7 %reduce-scatter.11.cloned.1.call-done = f32[64,1]{1,0:T(8,128)} async-done(((f32[1024,1]{1,0:T(8,128)}), f32[64,1]{1,0:T(8,128)}) %reduce-scatter.11.cloned.1.call-update) | async-done | bytes 272
  168.2 0.8 copy.43
  169.1 13.6 %all-reduce.2 = (f32[1,64]{1,0:T(1,128)S(1)}, f32[4,1,256]{2,0,1:T(4,128)S(1)}, f32[4,1]{0,1:T(1,128)S(1)}) all-reduce(f32[1,64]{1,0:T(1,128)S(1)} %copy.43, f32[4,1,256]{2,0,1:T(4,128)S(1)} %get-tuple-element.6, f32[4,1]{0,1:T(1,128)S(1)} %get-tuple-element.7), channel_id=5, replica_groups=mesh['sp_0'=16,'sp_1'=8,'tp'=8] {'sp_1'}, use_global_device_ids=true, to_apply=%region_10.11.clone | all-reduce | flops 1092 | bytes 8736
  182.7 0.8 fusion.46
  183.5 60.4 %reduce-scatter.7.cloned.1.call-done = f32[1,64,256]{2,1,0:T(8,128)} async-done(((f32[1,1024,256]{2,1,0:T(8,128)}), f32[1,64,256]{2,1,0:T(8,128)}) %reduce-scatter.7.cloned.1.call-update) | async-done | bytes 65552 | tf_op jit(solution)/shard_map/reduce_scatter | solution.py:25
  244.0 2.3 convolution_convert_fusion
  246.2 0.7 broadcast_in_dim.5
  246.9 15.2 %all-to-all-start = ((bf16[8,4,2048]{2,1,0:T(4,128)(2,1)}), bf16[8,4,2048]{2,1,0:T(4,128)(2,1)S(1)}, u32[]{:S(2)}, u32[]{:S(2)}) async-start(bf16[8,4,2048]{2,1,0:T(4,128)(2,1)} %broadcast_in_dim.5), calls=%async_computation.2 | async-start | bytes 262144 | tf_op jit(solution)/shard_map/all_to_all | solution.py:35
  262.2 1.3 dynamic-slice
  264.1 0.6 constant_dynamic-slice_fusion
  264.7 2.7 all-to-all-done
  267.4 0.7 reduce_sum.52
  268.1 25.5 %reduce-scatter.9.cloned.1.call-done = f32[1,8,256]{2,1,0:T(8,128)} async-done(((f32[1,64,256]{2,1,0:T(8,128)}), f32[1,8,256]{2,1,0:T(8,128)}) %reduce-scatter.9.cloned.1.call-update) | async-done | bytes 8208 | tf_op jit(solution)/shard_map/reduce_scatter | solution.py:25
  293.6 1.3 convert_element_type.97
  (18 shorter events, 0.1 us)
Async XLA Ops:
  7.2 1.6 copy-start
  7.2 3.0 copy-start.3
  7.2 161.1 %reduce-scatter.11.cloned.1.call-start = ((), (), s32[]{:S(2)}) async-start(), calls=%async_computation.6 | async-start | bytes 557056
  8.8 2.1 copy-start.4
  90.7 92.0 %copy-start.5 = (f32[4]{0:T(128)}, f32[4]{0:T(128)S(1)}, u32[]{:S(2)}) copy-start(f32[4]{0:T(128)S(1)} %max.44) | copy-start | bytes 52
  92.0 151.9 %reduce-scatter.7.cloned.1.call-start = ((), (), s32[]{:S(2)}) async-start(), calls=%async_computation.4 | async-start | bytes 1114112 | tf_op jit(solution)/shard_map/reduce_scatter | solution.py:25
  94.0 1.6 copy-start.2
  95.5 1.7 copy-start.1
  95.5 198.0 %reduce-scatter.9.cloned.1.call-start = ((), (), s32[]{:S(2)}) async-start(), calls=%async_computation.5 | async-start | bytes 73728 | tf_op jit(solution)/shard_map/reduce_scatter | solution.py:25
  246.9 20.5 %all-to-all-start = ((bf16[8,4,2048]{2,1,0:T(4,128)(2,1)}), bf16[8,4,2048]{2,1,0:T(4,128)(2,1)S(1)}, u32[]{:S(2)}, u32[]{:S(2)}) async-start(bf16[8,4,2048]{2,1,0:T(4,128)(2,1)} %broadcast_in_dim.5), calls=%async_computation.2 | async-start | bytes 262144 | tf_op jit(solution)/shard_map/all_to_all | solution.py:35
Sparse Core Ops, SparseCore 0:
  92.2 76.0 reduce-scatter.10
  171.6 72.2 reduce-scatter.6
  247.3 46.1 reduce-scatter.8
where the time goes:
time: 307 us; the launch traced here: 301 us
  waiting for transfers between devices  135 us (44%)
  blocking collectives  109 us (36%)
  starting transfers between devices  15.4 us (5%)
  matrix products  14.9 us (5%)
  between operations  14.6 us (5%)
  local copies, waits for them, and re-layouts  8.3 us (3%)
  other arithmetic  4.22 us (1%)
    reduce_scatter x2, waiting for transfers between devices, sum_by_axis(): nearer = lax.psum_scatter(value, axes[0], scatter_dimension=dim, tiled=True)  85.9 us
    all_gather x1, blocking collectives, sent_together(): lax.all_gather(both, axis, axis=dim, tiled=True)  73.7 us
    unnamed x4, waiting for transfers between devices  46.7 us
    psum x1, blocking collectives, by_axis(): return functools.reduce(lax.psum, axes, value)  21.3 us
    all_to_all x1, starting transfers between devices, copy_for_each(): lax.all_to_all(jnp.broadcast_to(value[None], (count, *value.shape)), axis...  15.2 us
    unnamed x1, blocking collectives  13.6 us
  transfers between devices with their start and end apart: 4, of which 4 were waited for; matrix products, arithmetic and copies ran while one was open for 5% of the time, Pallas kernels for 0%

commit v1 on v0

v1 whole, which is shorter than its diff:
```python
import functools

import jax
import jax.numpy as jnp
from jax import lax
from jax.experimental import pallas as pl
from jax.experimental.pallas import tpu as pltpu
from jax.sharding import Mesh
from jax.sharding import PartitionSpec as P

HD = 256
SP = ("sp_0", "sp_1")
LANES = 128
F32 = jnp.float32
BF16 = jnp.bfloat16

NT = (((1,), (1,)), ((), ()))
TN = (((0,), (0,)), ((), ()))


def parts3(x):
    hi = x.astype(BF16).astype(F32)
    rest = x - hi
    mid = rest.astype(BF16).astype(F32)
    return hi, mid, rest - mid


def log_sigmoid(x):
    return jnp.minimum(x, 0.0) - jnp.log1p(jnp.exp(-jnp.abs(x)))


def lanes_of(shape):
    return lax.broadcasted_iota(jnp.int32, shape, len(shape) - 1)


def row_of_head(w_ref, head):
    rows = lax.broadcasted_iota(jnp.int32, w_ref.shape, 0)
    picked = jnp.where(rows == head, w_ref[...].astype(F32), 0.0)
    return jnp.sum(picked, axis=0, keepdims=True)


def stat_rows(total, query_norm, peak):
    at = lanes_of(total.shape)
    packed = jnp.where(at < 4, total, jnp.where(at < 8, query_norm, peak))
    return jnp.concatenate(parts3(packed), axis=0)


def stats_from(rows):
    total = rows
    query_norm = pltpu.roll(rows, LANES - 4, 1)
    peak = pltpu.roll(rows, LANES - 8, 1)
    return total, query_norm, peak


def later_sums(total):
    later = [jnp.zeros_like(total[:1])]
    for i in range(total.shape[0] - 1, 0, -1):
        later.append(later[-1] + total[i : i + 1])
    later.reverse()
    return later


def block_kernel(
    seqs,
    n_y,
    tokens_ref,
    next_ref,
    w_query_ref,
    w_key_ref,
    w_value_ref,
    in_gate_ref,
    forget_gate_ref,
    bias_ref,
    decay_ref,
    out_ref,
):
    head = lax.axis_index("tp")
    span = tokens_ref.shape[0] // seqs
    scale = HD ** (-0.5)
    tokens = tokens_ref[...]
    keys = jnp.dot(tokens, w_key_ref[...], preferred_element_type=F32).astype(BF16)
    values = jnp.dot(tokens, w_value_ref[...], preferred_element_type=F32).astype(BF16)
    depth = tokens.shape[1]
    gate_rows = jnp.concatenate(
        [
            jnp.broadcast_to(row_of_head(in_gate_ref, head), (LANES, depth)),
            jnp.broadcast_to(row_of_head(forget_gate_ref, head), (LANES, depth)),
        ],
        axis=0,
    ).astype(BF16)
    gates = lax.dot_general(tokens, gate_rows, NT, preferred_element_type=F32)
    query = jnp.dot(next_ref[...], w_query_ref[...], preferred_element_type=F32).astype(BF16)

    prompt = lanes_of((span, LANES)) % seqs
    log_in = gates[:span, :LANES]
    forget = gates[:span, LANES:]
    for p in range(1, seqs):
        rows = slice(p * span, (p + 1) * span)
        log_in = jnp.where(prompt == p, gates[rows, :LANES], log_in)
        forget = jnp.where(prompt == p, gates[rows, LANES:], forget)
    decay = jnp.transpose(jnp.concatenate([decay_ref[...]] * (LANES // seqs), axis=0))
    log_forget = log_sigmoid(forget + bias_ref[head]) + decay
    after = (
        lax.broadcasted_iota(jnp.int32, (span, span), 1)
        > lax.broadcasted_iota(jnp.int32, (span, span), 0)
    ).astype(BF16)
    suffix = jnp.zeros((span, LANES), F32)
    for part in parts3(log_forget):
        suffix += jnp.dot(after, part.astype(BF16), preferred_element_type=F32)
    total = suffix[:1] + log_forget[:1]
    score = suffix + log_in
    peak = jnp.max(score, axis=0, keepdims=True)
    weight = jnp.exp(score - peak) * scale

    at = lanes_of((1, LANES)) % seqs
    query_norm = jnp.zeros((1, LANES), F32)
    ones = jnp.ones((8, span), BF16)
    high, low, norms = [], [], []
    run = HD // 4
    for p in range(seqs):
        rows = slice(p * span, (p + 1) * span)
        weighted = (keys[rows].astype(F32) * weight[:, p : p + 1]).astype(BF16)
        memory = lax.dot_general(weighted, values[rows], TN, preferred_element_type=F32)
        norms.append(jnp.dot(ones, weighted, preferred_element_type=F32)[:1])
        along = lax.dot_general(query, weighted, NT, preferred_element_type=F32)[p : p + 1]
        query_norm = jnp.where(at == p, jnp.sum(along, axis=1, keepdims=True), query_norm)
        stacked = jnp.concatenate(parts3(along) + (jnp.zeros((5, span), F32),), axis=0)
        reads = jnp.dot(stacked.astype(BF16), values[rows], preferred_element_type=F32)
        read = jnp.sum(reads, axis=0, keepdims=True)
        read_high = read.astype(BF16).astype(F32)
        high.append(read_high)
        low.append(read - read_high)
        for y in range(n_y):
            pieces = [memory[r * run + y * 8 : r * run + y * 8 + 8] for r in range(4)]
            out_ref[y, p * 32 : (p + 1) * 32, :] = jnp.concatenate(pieces, axis=0).astype(BF16)
    stats = stat_rows(total, query_norm, peak)
    wide = jnp.concatenate([stats, jnp.zeros_like(stats)], axis=1)
    extra = jnp.concatenate(high + low + norms + [wide, jnp.zeros((1, HD), F32)], axis=0)
    extra = extra.astype(BF16)
    for y in range(n_y):
        out_ref[y, 128:144, :] = extra


def group_kernel(seqs, n_y, n_z, in_ref, out_ref):
    extras = [in_ref[y, 128:144, :].astype(F32) for y in range(n_y)]
    rows = jnp.concatenate(
        [e[12:13, :LANES] + e[13:14, :LANES] + e[14:15, :LANES] for e in extras], axis=0
    )
    total, query_norm, peak = stats_from(rows)
    later = later_sums(total)
    scores = [later[y] + peak[y : y + 1] for y in range(n_y)]
    group_total = later[0] + total[:1]
    group_peak = functools.reduce(jnp.maximum, scores)
    coef = jnp.exp(jnp.concatenate(scores, axis=0) - group_peak)
    group_norm = jnp.sum(coef * query_norm, axis=0, keepdims=True)
    tall = jnp.transpose(jnp.concatenate([coef] * (LANES // n_y), axis=0))
    per_y = [jnp.broadcast_to(tall[:8, y : y + 1], (8, HD)) for y in range(n_y)]

    at = lanes_of((1, LANES))
    stats = stat_rows(
        group_total, pltpu.roll(jnp.broadcast_to(group_norm, (8, LANES)), 4, 1)[:1],
        pltpu.roll(jnp.broadcast_to(group_peak, (8, LANES)), 8, 1)[:1],
    )
    stats = jnp.where(at < 12, stats, 0.0)
    wide = jnp.concatenate([stats, jnp.zeros_like(stats)], axis=1)
    reads = jnp.zeros((seqs, HD), F32)
    norms = jnp.zeros((seqs, HD), F32)
    for y in range(n_y):
        c = per_y[y][:seqs]
        e = extras[y]
        reads += c * (e[:seqs] + e[seqs : 2 * seqs])
        norms += c * e[2 * seqs : 3 * seqs]
    for p in range(seqs):
        memory = jnp.zeros((32, HD), F32)
        for y in range(n_y):
            memory += per_y[y][p : p + 1] * in_ref[y, p * 32 : (p + 1) * 32, :].astype(F32)
        tail = jnp.concatenate([reads, wide, norms[p : p + 1]], axis=0)
        for r in range(n_z // seqs):
            block = jnp.concatenate([memory[r * 8 : r * 8 + 8], tail], axis=0)
            out_ref[p * (n_z // seqs) + r] = block.astype(BF16)


def final_kernel(
    seqs,
    n_z,
    n_tp,
    in_ref,
    query_ref,
    key_ref,
    value_ref,
    new_in_ref,
    new_forget_ref,
    w_out_ref,
    memory_ref,
    norm_ref,
    stab_ref,
    head_ref,
):
    z = lax.axis_index("sp_0")
    y = lax.axis_index("sp_1")
    per_prompt = n_z // seqs
    mine = z // per_prompt
    blocks = [in_ref[i].astype(F32) for i in range(n_z)]
    rows = jnp.concatenate(
        [b[12:13, :LANES] + b[13:14, :LANES] + b[14:15, :LANES] for b in blocks], axis=0
    )
    total, query_norm, peak = stats_from(rows)
    later = later_sums(total)
    scores = [later[i] + peak[i : i + 1] for i in range(n_z)]
    stab = functools.reduce(jnp.maximum, scores, later[0] + total[:1])
    coef = jnp.exp(jnp.concatenate(scores, axis=0) - stab)
    all_norm = jnp.sum(coef * query_norm, axis=0, keepdims=True)
    filled = jnp.zeros((LANES - n_z - 2, LANES), F32)
    tall = jnp.transpose(jnp.concatenate([coef, stab, all_norm, filled], axis=0))[:8]
    stab4 = tall[:seqs, n_z : n_z + 1]
    query_norm4 = tall[:seqs, n_z + 1 : n_z + 2]
    stab_ref[...] = stab4

    is_mine = lanes_of(coef.shape) == mine
    own = jnp.sum(jnp.where(is_mine, coef, 0.0), axis=1, keepdims=True)
    memory = jnp.zeros((8, HD), F32)
    norm = jnp.zeros((1, HD), F32)
    query_state = jnp.zeros((seqs, HD), F32)
    for i in range(n_z):
        memory += own[i : i + 1] * blocks[i][:8]
        norm += own[i : i + 1] * blocks[i][15:16]
        query_state += tall[:seqs, i : i + 1] * blocks[i][8:12]
    memory_ref[...] = memory.astype(BF16)
    first = lax.rem(z, per_prompt) * (HD // per_prompt) + y * 8
    turned = pltpu.roll(jnp.broadcast_to(norm, (8, HD)), lax.rem(HD - first, HD), 1)
    norm_ref[...] = turned[:1, :8]

    query = query_ref[...]
    new_key = key_ref[...]
    new_value = value_ref[...]
    new_in = new_in_ref[...]
    carried = new_forget_ref[...] + stab4
    top = jnp.maximum(carried, new_in)
    keep = jnp.exp(carried - top)
    take = jnp.exp(new_in - top)
    qk = jnp.sum(query * new_key, axis=1, keepdims=True)
    numer = keep * query_state + take * qk * new_value
    denom = keep * query_norm4 + take * qk
    head_out = (numer / jnp.maximum(jnp.abs(denom), 1.0)).astype(BF16)
    partial = jnp.dot(head_out, w_out_ref[...], preferred_element_type=F32).astype(BF16)
    for i in range(n_tp):
        head_ref[i] = partial


def per_device(
    tokens,
    next_tokens,
    w_query,
    w_key,
    w_value,
    w_in_gate,
    w_forget_gate,
    forget_bias,
    extra_decay,
    w_out,
):
    scale = HD ** (-0.5)
    seqs, span, depth = tokens.shape
    n_z, n_y, n_tp = (lax.axis_size(a) for a in ("sp_0", "sp_1", "tp"))
    whole = pl.BlockSpec(memory_space=pltpu.VMEM)
    scalar = pl.BlockSpec(memory_space=pltpu.SMEM)

    sent = pl.pallas_call(
        functools.partial(block_kernel, seqs, n_y),
        out_shape=jax.ShapeDtypeStruct((n_y, 144, HD), BF16),
        in_specs=[whole] * 7 + [scalar, whole],
        out_specs=whole,
        cost_estimate=pl.CostEstimate(
            flops=2 * seqs * span * depth * 3 * HD, bytes_accessed=6 << 20, transcendentals=0
        ),
    )(
        tokens.reshape(seqs * span, depth),
        next_tokens,
        w_query,
        w_key,
        w_value,
        w_in_gate.T,
        w_forget_gate.T,
        forget_bias,
        extra_decay.reshape(seqs, span),
    )
    arrived = lax.all_to_all(sent, "sp_1", 0, 0, tiled=True)

    head = lax.axis_index("tp")
    gate_in = lax.dynamic_slice_in_dim(w_in_gate, head, 1, 1)
    gate_forget = lax.dynamic_slice_in_dim(w_forget_gate, head, 1, 1)
    bias_here = lax.dynamic_slice_in_dim(forget_bias, head, 1, 0)

    def rounded(w):
        return jnp.dot(next_tokens, w, preferred_element_type=F32).astype(BF16).astype(F32)

    query = rounded(w_query)
    new_key = rounded(w_key) * scale
    new_value = rounded(w_value)
    new_in = jnp.dot(next_tokens, gate_in, preferred_element_type=F32)
    new_forget = jax.nn.log_sigmoid(
        jnp.dot(next_tokens, gate_forget, preferred_element_type=F32) + bias_here
    )

    group = pl.pallas_call(
        functools.partial(group_kernel, seqs, n_y, n_z),
        out_shape=jax.ShapeDtypeStruct((n_z, 16, HD), BF16),
        in_specs=[whole],
        out_specs=whole,
    )(arrived)
    gathered = lax.all_to_all(group, "sp_0", 0, 0, tiled=True)

    memory, norm, stab, partial = pl.pallas_call(
        functools.partial(final_kernel, seqs, n_z, n_tp),
        out_shape=(
            jax.ShapeDtypeStruct((8, HD), BF16),
            jax.ShapeDtypeStruct((1, 8), F32),
            jax.ShapeDtypeStruct((seqs, 1), F32),
            jax.ShapeDtypeStruct((n_tp, seqs, depth), BF16),
        ),
        in_specs=[whole] * 7,
        out_specs=(whole,) * 4,
    )(gathered, query, new_key, new_value, new_in, new_forget, w_out)
    parts = lax.all_to_all(partial, "tp", 0, 0, tiled=True)
    read = parts.astype(F32).sum(axis=0).astype(BF16)
    return memory[None], norm, stab, read


def solution(mesh):
    torus = Mesh(mesh.devices.reshape(16, 8, mesh.shape["tp"]), ("sp_0", "sp_1", "tp"))
    placed = (
        P(None, SP, None),
        P(),
        P(None, "tp"),
        P(None, "tp"),
        P(None, "tp"),
        P(),
        P(),
        P(),
        P("tp", None, SP),
        P("tp", None),
    )
    return jax.shard_map(
        per_device,
        mesh=torus,
        in_specs=placed,
        out_specs=(P("tp", SP, None), P("tp", SP), P(None, "tp"), P()),
        check_vma=False,
    )
```

time: 307 us -> 85.8 us (0.28); the launches traced: 301 us -> 85.2 us
  waiting for transfers between devices: 135 us -> 20.7 us
  blocking collectives: 109 us -> 0 us
  starting transfers between devices: 15.4 us -> 40.5 us
  between operations: 14.6 us -> 0.69 us
  Pallas kernels: 0 us -> 11.8 us
  matrix products: 14.9 us -> 6.77 us
  local copies, waits for them, and re-layouts: 8.3 us -> 4.01 us
  other arithmetic: 4.22 us -> 0.67 us
    reduce_scatter x2 -> x0, waiting for transfers between devices: 85.9 us -> none  [sum_by_axis(): nearer = lax.psum_scatter(value, axes[0], scatter_dimension=dim, tiled=True)]
    all_gather x1 -> x0, blocking collectives: 73.7 us -> none  [sent_together(): lax.all_gather(both, axis, axis=dim, tiled=True)]
    unnamed x4 -> x0, waiting for transfers between devices: 46.7 us -> none
    all_to_all x1 -> x3, starting transfers between devices: 15.2 us -> 40.5 us  [the longest x1 25.1 us: per_device(): gathered = lax.all_to_all(group, 'sp_0', 0, 0, tiled=True)]
    psum x1 -> x0, blocking collectives: 21.3 us -> none  [by_axis(): return functools.reduce(lax.psum, axes, value)]
    all_to_all x1 -> x3, waiting for transfers between devices: 2.74 us -> 20.7 us  [the longest x1 9.08 us: per_device(): gathered = lax.all_to_all(group, 'sp_0', 0, 0, tiled=True)]
    unnamed x1 -> x0, blocking collectives: 13.6 us -> none
    pallas_call x0 -> x3, Pallas kernels: none -> 11.8 us  [the longest x1 7.09 us: per_device(): pl.pallas_call(functools.partial(block_kernel, seqs, n_y), out_shape=jax....]
  transfers between devices with their start and end apart: 4 -> 3, of which waited for: 4 -> 3; matrix products, arithmetic and copies ran while one was open for 5% -> 11% of each run, Pallas kernels for 0% -> 0%
where the time goes in v1:
time: 85.8 us; the launch traced here: 85.2 us
  starting transfers between devices  40.5 us (47%)
  waiting for transfers between devices  20.7 us (24%)
  Pallas kernels  11.8 us (14%)
  matrix products  6.77 us (8%)
  local copies, waits for them, and re-layouts  4.01 us (5%)
    all_to_all x1, starting transfers between devices, per_device(): gathered = lax.all_to_all(group, 'sp_0', 0, 0, tiled=True)  25.1 us
    all_to_all x1, waiting for transfers between devices, per_device(): gathered = lax.all_to_all(group, 'sp_0', 0, 0, tiled=True)  9.08 us
    all_to_all x1, starting transfers between devices, per_device(): arrived = lax.all_to_all(sent, 'sp_1', 0, 0, tiled=True)  7.77 us
    all_to_all x1, waiting for transfers between devices, per_device(): arrived = lax.all_to_all(sent, 'sp_1', 0, 0, tiled=True)  7.69 us
    all_to_all x1, starting transfers between devices, per_device(): parts = lax.all_to_all(partial, 'tp', 0, 0, tiled=True)  7.66 us
    pallas_call x1, Pallas kernels, per_device(): pl.pallas_call(functools.partial(block_kernel, seqs, n_y), out_shape=jax....  7.09 us
    all_to_all x1, waiting for transfers between devices, per_device(): parts = lax.all_to_all(partial, 'tp', 0, 0, tiled=True)  3.97 us
    dot_general x3, matrix products, rounded(): jnp.dot(next_tokens, w, preferred_element_type=F32).astype(BF16).astype(F32)  3.75 us
  transfers between devices with their start and end apart: 3, of which 3 were waited for; matrix products, arithmetic and copies ran while one was open for 11% of the time, Pallas kernels for 0%

profile of v1, /device:TPU:1, one launch (start us, length us, event | category | flops | bytes accessed | tf_op | source)
XLA Modules:
  0.0 85.2 jit_solution(8804765616613800049)
XLA Ops:
  0.6 0.0 copy-start.5
  0.6 0.0 copy-start.4
  0.7 0.0 copy-start.1
  0.7 7.1 %shard_map.129 = bf16[8,144,256]{2,1,0:T(8,128)(2,1)} custom-call(bf16[512,2048]{1,0:T(8,128)(2,1)} %bitcast.30, bf16[4,2048]{1,0:T(4,128)(2,1)} %next_ref.1, bf16[2048,256]{1,0:T(8,128)(2,1)} %w_query_ref.1, bf16[2048,256]{1,0:T(8,128)(2,1)} %w_key_ref.1, bf16[2048,256]{1,0:T(8,128)(2,1)} %w_value_ref.1, bf16[8,2048]{1,0:T(8,128)(2,1)} %bitcast.32, ...), custom_call_target="tpu_custom_call" | custom-call | flops 1610612736 | bytes 6291456 | tf_op jit(solution)/shard_map/pallas_call | solution.py:268
  7.8 0.0 copy-start.2
  7.8 7.8 %all-to-all-start = ((bf16[8,144,256]{2,1,0:T(8,128)(2,1)}), bf16[8,144,256]{2,1,0:T(8,128)(2,1)S(1)}, u32[]{:S(2)}, u32[]{:S(2)}) async-start(bf16[8,144,256]{2,1,0:T(8,128)(2,1)} %shard_map.129), calls=%async_computation | async-start | bytes 1179648 | tf_op jit(solution)/shard_map/all_to_all | solution.py:287
  15.5 0.0 copy-done.5
  15.5 0.6 dynamic_slice.11
  16.1 0.0 copy-done.4
  16.1 1.5 %fusion.11 = f32[4,1]{0,1:T(1,128)S(1)} fusion(bf16[4,2048]{1,0:T(4,128)(2,1)S(1)} %copy-done.4, bf16[2048,8]{0,1:T(8,128)(2,1)} %param.16, s32[]{:T(128)S(6)} %select_n.11, f32[]{:T(128)} %bitcast.7), kind=kOutput, calls=%fused_computation.15 | convolution fusion | flops 16420 | bytes 25108 | tf_op jit(solution)/shard_map/dot_general | solution.py:302
  17.7 0.7 copy.15.new_forget_ref
  18.4 1.5 %convolution_bitcast_fusion.new_in_ref = f32[4,1]{1,0:T(4,128)} fusion(bf16[4,2048]{1,0:T(4,128)(2,1)S(1)} %copy-done.4, bf16[2048,8]{0,1:T(8,128)(2,1)} %param.15, s32[]{:T(128)S(6)} %select_n.11), kind=kOutput, calls=%fused_computation.7 | convolution fusion | flops 16384 | bytes 24596 | tf_op jit(solution)/shard_map/dot_general | solution.py:300
  19.8 0.0 copy-done.1
  19.8 0.8 fusion.3.query_ref
  20.7 7.7 %all-to-all-done.in_ref = bf16[8,144,256]{2,1,0:T(8,128)(2,1)S(1)} async-done(((bf16[8,144,256]{2,1,0:T(8,128)(2,1)}), bf16[8,144,256]{2,1,0:T(8,128)(2,1)S(1)}, u32[]{:S(2)}, u32[]{:S(2)}) %all-to-all-start) | async-done | bytes 589856 | tf_op jit(solution)/shard_map/all_to_all | solution.py:287
  28.4 0.0 copy-start
  28.4 0.8 copy-done
  29.2 2.1 %shard_map.130 = bf16[16,16,256]{2,1,0:T(8,128)(2,1)} custom-call(bf16[8,144,256]{2,1,0:T(8,128)(2,1)} %copy-done), custom_call_target="tpu_custom_call" | custom-call | tf_op jit(solution)/shard_map/pallas_call | solution.py:305
  31.3 25.1 %all-to-all-start.1 = ((bf16[16,16,256]{2,1,0:T(8,128)(2,1)}), bf16[16,16,256]{2,1,0:T(8,128)(2,1)S(1)}, u32[]{:S(2)}, u32[]{:S(2)}) async-start(bf16[16,16,256]{2,1,0:T(8,128)(2,1)} %shard_map.130), calls=%async_computation.1 | async-start | bytes 262144 | tf_op jit(solution)/shard_map/all_to_all | solution.py:311
  56.4 0.0 copy-done.2
  56.4 0.8 fusion.2.key_ref
  57.3 2.1 %fusion.value_ref = f32[4,256]{1,0:T(4,128)} fusion(bf16[4,2048]{1,0:T(4,128)(2,1)S(1)} %copy-done.4, bf16[2048,256]{1,0:T(8,128)(2,1)} %w_value_ref.1), kind=kOutput, calls=%fused_computation.1 | convolution fusion | flops 4196352 | bytes 1069056 | tf_op jit(solution)/shard_map/dot_general | solution.py:295
  59.3 9.1 %all-to-all-done.1.in_ref = bf16[16,16,256]{2,1,0:T(8,128)(2,1)S(1)} async-done(((bf16[16,16,256]{2,1,0:T(8,128)(2,1)}), bf16[16,16,256]{2,1,0:T(8,128)(2,1)S(1)}, u32[]{:S(2)}, u32[]{:S(2)}) %all-to-all-start.1) | async-done | bytes 131104 | tf_op jit(solution)/shard_map/all_to_all | solution.py:311
  68.4 0.0 copy-start.3
  68.4 0.6 copy-done.3
  69.0 2.6 %shard_map.131 = (bf16[8,256]{1,0:T(8,128)(2,1)}, f32[1,8]{1,0:T(1,128)}, f32[4,1]{1,0:T(4,128)}, bf16[8,4,2048]{2,1,0:T(4,128)(2,1)}) custom-call(bf16[16,16,256]{2,1,0:T(8,128)(2,1)} %copy-done.3, f32[4,256]{1,0:T(4,128)} %fusion.3.query_ref, f32[4,256]{1,0:T(4,128)} %fusion.2.key_ref, f32[4,256]{1,0:T(4,128)} %fusion.value_ref, ...), custom_call_target="tpu_custom_call" | custom-call | tf_op jit(solution)/shard_map/pallas_call | solution.py:313
  71.6 7.7 %all-to-all-start.2 = ((bf16[8,4,2048]{2,1,0:T(4,128)(2,1)}), bf16[8,4,2048]{2,1,0:T(4,128)(2,1)S(1)}, u32[]{:S(2)}, u32[]{:S(2)}) async-start(bf16[8,4,2048]{2,1,0:T(4,128)(2,1)} %get-tuple-element.11), calls=%async_computation.2 | async-start | bytes 262144 | tf_op jit(solution)/shard_map/all_to_all | solution.py:324
  79.3 1.3 %copy.16 = f32[4,1]{0,1:T(1,128)} copy(f32[4,1]{1,0:T(4,128)} %get-tuple-element.14) | data formatting | bytes 32
  80.6 4.0 %all-to-all-done.2 = bf16[8,4,2048]{2,1,0:T(4,128)(2,1)S(1)} async-done(((bf16[8,4,2048]{2,1,0:T(4,128)(2,1)}), bf16[8,4,2048]{2,1,0:T(4,128)(2,1)S(1)}, u32[]{:S(2)}, u32[]{:S(2)}) %all-to-all-start.2) | async-done | bytes 131104 | tf_op jit(solution)/shard_map/all_to_all | solution.py:324
  84.5 0.7 reduce_sum.12
Async XLA Ops:
  0.6 14.9 %copy-start.5 = (f32[8]{0:T(128)S(1)}, f32[8]{0:T(128)}, u32[]{:S(2)}) copy-start(f32[8]{0:T(128)} %bias_ref.1) | copy-start | bytes 100
  0.6 15.5 %copy-start.4 = (bf16[4,2048]{1,0:T(4,128)(2,1)S(1)}, bf16[4,2048]{1,0:T(4,128)(2,1)}, u32[]{:S(2)}) copy-start(bf16[4,2048]{1,0:T(4,128)(2,1)} %next_ref.1) | copy-start | bytes 49156
  0.7 19.2 %copy-start.1 = (bf16[2048,256]{1,0:T(8,128)(2,1)S(1)}, bf16[2048,256]{1,0:T(8,128)(2,1)}, u32[]{:S(2)}) copy-start(bf16[2048,256]{1,0:T(8,128)(2,1)} %w_query_ref.1) | copy-start | bytes 3145732
  7.8 48.7 %copy-start.2 = (bf16[2048,256]{1,0:T(8,128)(2,1)S(1)}, bf16[2048,256]{1,0:T(8,128)(2,1)}, u32[]{:S(2)}) copy-start(bf16[2048,256]{1,0:T(8,128)(2,1)} %w_key_ref.1) | copy-start | bytes 3145732
  7.8 20.6 %all-to-all-start = ((bf16[8,144,256]{2,1,0:T(8,128)(2,1)}), bf16[8,144,256]{2,1,0:T(8,128)(2,1)S(1)}, u32[]{:S(2)}, u32[]{:S(2)}) async-start(bf16[8,144,256]{2,1,0:T(8,128)(2,1)} %shard_map.129), calls=%async_computation | async-start | bytes 1179648 | tf_op jit(solution)/shard_map/all_to_all | solution.py:287
  28.4 0.8 copy-start
  31.3 37.1 %all-to-all-start.1 = ((bf16[16,16,256]{2,1,0:T(8,128)(2,1)}), bf16[16,16,256]{2,1,0:T(8,128)(2,1)S(1)}, u32[]{:S(2)}, u32[]{:S(2)}) async-start(bf16[16,16,256]{2,1,0:T(8,128)(2,1)} %shard_map.130), calls=%async_computation.1 | async-start | bytes 262144 | tf_op jit(solution)/shard_map/all_to_all | solution.py:311
  68.4 0.6 copy-start.3
  71.6 12.9 %all-to-all-start.2 = ((bf16[8,4,2048]{2,1,0:T(4,128)(2,1)}), bf16[8,4,2048]{2,1,0:T(4,128)(2,1)S(1)}, u32[]{:S(2)}, u32[]{:S(2)}) async-start(bf16[8,4,2048]{2,1,0:T(4,128)(2,1)} %get-tuple-element.11), calls=%async_computation.2 | async-start | bytes 262144 | tf_op jit(solution)/shard_map/all_to_all | solution.py:324

commit v2 on v1

--- a/solution.py
+++ b/solution.py
@@ -33,23 +33,8 @@
     return lax.broadcasted_iota(jnp.int32, shape, len(shape) - 1)
 
 
-def row_of_head(w_ref, head):
-    rows = lax.broadcasted_iota(jnp.int32, w_ref.shape, 0)
-    picked = jnp.where(rows == head, w_ref[...].astype(F32), 0.0)
-    return jnp.sum(picked, axis=0, keepdims=True)
-
-
-def stat_rows(total, query_norm, peak):
-    at = lanes_of(total.shape)
-    packed = jnp.where(at < 4, total, jnp.where(at < 8, query_norm, peak))
-    return jnp.concatenate(parts3(packed), axis=0)
-
-
 def stats_from(rows):
-    total = rows
-    query_norm = pltpu.roll(rows, LANES - 4, 1)
-    peak = pltpu.roll(rows, LANES - 8, 1)
-    return total, query_norm, peak
+    return rows, pltpu.roll(rows, LANES - 4, 1), pltpu.roll(rows, LANES - 8, 1)
 
 
 def later_sums(total):
@@ -63,82 +48,121 @@
 def block_kernel(
     seqs,
     n_y,
+    tokens_hbm,
+    next_hbm,
+    w_query_hbm,
+    w_key_hbm,
+    w_value_hbm,
+    in_gate_hbm,
+    forget_gate_hbm,
+    bias_hbm,
+    decay_hbm,
+    out_hbm,
     tokens_ref,
     next_ref,
     w_query_ref,
     w_key_ref,
     w_value_ref,
-    in_gate_ref,
-    forget_gate_ref,
+    gate_ref,
     bias_ref,
     decay_ref,
     out_ref,
+    sems,
+    out_sems,
 ):
     head = lax.axis_index("tp")
+    depth = tokens_ref.shape[1]
+    heads = in_gate_hbm.shape[0]
     span = tokens_ref.shape[0] // seqs
     scale = HD ** (-0.5)
-    tokens = tokens_ref[...]
-    keys = jnp.dot(tokens, w_key_ref[...], preferred_element_type=F32).astype(BF16)
-    values = jnp.dot(tokens, w_value_ref[...], preferred_element_type=F32).astype(BF16)
-    depth = tokens.shape[1]
-    gate_rows = jnp.concatenate(
-        [
-            jnp.broadcast_to(row_of_head(in_gate_ref, head), (LANES, depth)),
-            jnp.broadcast_to(row_of_head(forget_gate_ref, head), (LANES, depth)),
-        ],
-        axis=0,
+    moves = [
+        (in_gate_hbm, gate_ref.at[pl.ds(0, heads)]),
+        (forget_gate_hbm, gate_ref.at[pl.ds(heads, heads)]),
+        (tokens_hbm, tokens_ref),
+        (bias_hbm, bias_ref),
+        (decay_hbm, decay_ref),
+        (w_key_hbm, w_key_ref),
+        (next_hbm, next_ref),
+        (w_query_hbm, w_query_ref),
+        (w_value_hbm, w_value_ref),
+    ]
+    copies = [pltpu.make_async_copy(a, b, sems.at[i]) for i, (a, b) in enumerate(moves)]
+    for copy in copies:
+        copy.start()
+    after = (
+        lax.broadcasted_iota(jnp.int32, (span, span), 0)
+        > lax.broadcasted_iota(jnp.int32, (span, span), 1)
     ).astype(BF16)
-    gates = lax.dot_general(tokens, gate_rows, NT, preferred_element_type=F32)
+
+    for copy in copies:
+        copy.wait()
+    gates = lax.dot_general(gate_ref[...], tokens_ref[...], NT, preferred_element_type=F32)
+    row = lax.broadcasted_iota(jnp.int32, gates.shape, 0)
+    log_in = jnp.sum(jnp.where(row == head, gates, 0.0), axis=0, keepdims=True)
+    forget = jnp.sum(jnp.where(row == head + heads, gates, 0.0), axis=0, keepdims=True)
+    log_in, forget = (
+        jnp.concatenate([v[:, p * span : (p + 1) * span] for p in range(seqs)], axis=0)
+        for v in (log_in, forget)
+    )
+    log_forget = log_sigmoid(forget + bias_ref[head]) + decay_ref[...]
+    split = jnp.concatenate(parts3(log_forget) + (jnp.zeros((seqs, span), F32),), axis=0)
+    sums = jnp.dot(split.astype(BF16), after, preferred_element_type=F32)
+    suffix = sums[:seqs] + sums[seqs : 2 * seqs] + sums[2 * seqs : 3 * seqs]
+    total = jnp.sum(log_forget, axis=1, keepdims=True)
+    score = suffix + log_in
+    peak = jnp.max(score, axis=1, keepdims=True)
+    weight = jnp.exp(score - peak) * scale
+    stats = [jnp.broadcast_to(v, (seqs, span)) for v in (total, peak)]
+    fill = jnp.zeros((LANES - 3 * seqs, span), F32)
+    turned = jnp.transpose(jnp.concatenate([weight] + stats + [fill], axis=0))
+
+    keys = jnp.dot(tokens_ref[...], w_key_ref[...], preferred_element_type=F32)
+    weighted = []
+    for p in range(seqs):
+        rows = slice(p * span, (p + 1) * span)
+        rounded = keys[rows].astype(BF16).astype(F32)
+        weighted.append((rounded * turned[:, p : p + 1]).astype(BF16))
+
     query = jnp.dot(next_ref[...], w_query_ref[...], preferred_element_type=F32).astype(BF16)
-
-    prompt = lanes_of((span, LANES)) % seqs
-    log_in = gates[:span, :LANES]
-    forget = gates[:span, LANES:]
-    for p in range(1, seqs):
-        rows = slice(p * span, (p + 1) * span)
-        log_in = jnp.where(prompt == p, gates[rows, :LANES], log_in)
-        forget = jnp.where(prompt == p, gates[rows, LANES:], forget)
-    decay = jnp.transpose(jnp.concatenate([decay_ref[...]] * (LANES // seqs), axis=0))
-    log_forget = log_sigmoid(forget + bias_ref[head]) + decay
-    after = (
-        lax.broadcasted_iota(jnp.int32, (span, span), 1)
-        > lax.broadcasted_iota(jnp.int32, (span, span), 0)
-    ).astype(BF16)
-    suffix = jnp.zeros((span, LANES), F32)
-    for part in parts3(log_forget):
-        suffix += jnp.dot(after, part.astype(BF16), preferred_element_type=F32)
-    total = suffix[:1] + log_forget[:1]
-    score = suffix + log_in
-    peak = jnp.max(score, axis=0, keepdims=True)
-    weight = jnp.exp(score - peak) * scale
-
-    at = lanes_of((1, LANES)) % seqs
-    query_norm = jnp.zeros((1, LANES), F32)
+    values = jnp.dot(tokens_ref[...], w_value_ref[...], preferred_element_type=F32).astype(BF16)
+    at = lanes_of((1, LANES))
+    stats = jnp.where(at < seqs, 0.0, turned[:1])
     ones = jnp.ones((8, span), BF16)
-    high, low, norms = [], [], []
+    high, low, norms, sends = [], [], [], []
     run = HD // 4
     for p in range(seqs):
         rows = slice(p * span, (p + 1) * span)
-        weighted = (keys[rows].astype(F32) * weight[:, p : p + 1]).astype(BF16)
-        memory = lax.dot_general(weighted, values[rows], TN, preferred_element_type=F32)
-        norms.append(jnp.dot(ones, weighted, preferred_element_type=F32)[:1])
-        along = lax.dot_general(query, weighted, NT, preferred_element_type=F32)[p : p + 1]
-        query_norm = jnp.where(at == p, jnp.sum(along, axis=1, keepdims=True), query_norm)
+        memory = lax.dot_general(weighted[p], values[rows], TN, preferred_element_type=F32)
+        for y in range(n_y):
+            pieces = [memory[r * run + y * 8 : r * run + y * 8 + 8] for r in range(4)]
+            out_ref[y, p * 32 : (p + 1) * 32, :] = jnp.concatenate(pieces, axis=0).astype(BF16)
+        part = pl.ds(p * 32, 32)
+        sends.append(
+            pltpu.make_async_copy(out_ref.at[:, part, :], out_hbm.at[:, part, :], out_sems.at[p])
+        )
+        sends[-1].start()
+        norms.append(jnp.dot(ones, weighted[p], preferred_element_type=F32)[:1])
+        along = lax.dot_general(query, weighted[p], NT, preferred_element_type=F32)[p : p + 1]
+        stats = jnp.where(at == p, jnp.sum(along, axis=1, keepdims=True), stats)
         stacked = jnp.concatenate(parts3(along) + (jnp.zeros((5, span), F32),), axis=0)
         reads = jnp.dot(stacked.astype(BF16), values[rows], preferred_element_type=F32)
         read = jnp.sum(reads, axis=0, keepdims=True)
         read_high = read.astype(BF16).astype(F32)
         high.append(read_high)
         low.append(read - read_high)
-        for y in range(n_y):
-            pieces = [memory[r * run + y * 8 : r * run + y * 8 + 8] for r in range(4)]
-            out_ref[y, p * 32 : (p + 1) * 32, :] = jnp.concatenate(pieces, axis=0).astype(BF16)
-    stats = stat_rows(total, query_norm, peak)
+    stats = jnp.concatenate(parts3(stats), axis=0)
     wide = jnp.concatenate([stats, jnp.zeros_like(stats)], axis=1)
     extra = jnp.concatenate(high + low + norms + [wide, jnp.zeros((1, HD), F32)], axis=0)
     extra = extra.astype(BF16)
     for y in range(n_y):
         out_ref[y, 128:144, :] = extra
+    part = pl.ds(128, 16)
+    sends.append(
+        pltpu.make_async_copy(out_ref.at[:, part, :], out_hbm.at[:, part, :], out_sems.at[seqs])
+    )
+    sends[-1].start()
+    for copy in sends:
+        copy.wait()
 
 
 def group_kernel(seqs, n_y, n_z, in_ref, out_ref):
@@ -146,7 +170,7 @@
     rows = jnp.concatenate(
         [e[12:13, :LANES] + e[13:14, :LANES] + e[14:15, :LANES] for e in extras], axis=0
     )
-    total, query_norm, peak = stats_from(rows)
+    query_norm, total, peak = stats_from(rows)
     later = later_sums(total)
     scores = [later[y] + peak[y : y + 1] for y in range(n_y)]
     group_total = later[0] + total[:1]
@@ -157,11 +181,10 @@
     per_y = [jnp.broadcast_to(tall[:8, y : y + 1], (8, HD)) for y in range(n_y)]
 
     at = lanes_of((1, LANES))
-    stats = stat_rows(
-        group_total, pltpu.roll(jnp.broadcast_to(group_norm, (8, LANES)), 4, 1)[:1],
-        pltpu.roll(jnp.broadcast_to(group_peak, (8, LANES)), 8, 1)[:1],
-    )
-    stats = jnp.where(at < 12, stats, 0.0)
+    total_there = pltpu.roll(jnp.broadcast_to(group_total, (8, LANES)), 4, 1)[:1]
+    peak_there = pltpu.roll(jnp.broadcast_to(group_peak, (8, LANES)), 8, 1)[:1]
+    packed = jnp.where(at < 4, group_norm, jnp.where(at < 8, total_there, peak_there))
+    stats = jnp.concatenate(parts3(jnp.where(at < 12, packed, 0.0)), axis=0)
     wide = jnp.concatenate([stats, jnp.zeros_like(stats)], axis=1)
     reads = jnp.zeros((seqs, HD), F32)
     norms = jnp.zeros((seqs, HD), F32)
@@ -204,7 +227,7 @@
     rows = jnp.concatenate(
         [b[12:13, :LANES] + b[13:14, :LANES] + b[14:15, :LANES] for b in blocks], axis=0
     )
-    total, query_norm, peak = stats_from(rows)
+    query_norm, total, peak = stats_from(rows)
     later = later_sums(total)
     scores = [later[i] + peak[i : i + 1] for i in range(n_z)]
     stab = functools.reduce(jnp.maximum, scores, later[0] + total[:1])
@@ -263,13 +286,27 @@
     seqs, span, depth = tokens.shape
     n_z, n_y, n_tp = (lax.axis_size(a) for a in ("sp_0", "sp_1", "tp"))
     whole = pl.BlockSpec(memory_space=pltpu.VMEM)
-    scalar = pl.BlockSpec(memory_space=pltpu.SMEM)
+    heads = w_in_gate.shape[1]
+    hbm = pl.BlockSpec(memory_space=pl.ANY)
 
     sent = pl.pallas_call(
         functools.partial(block_kernel, seqs, n_y),
         out_shape=jax.ShapeDtypeStruct((n_y, 144, HD), BF16),
-        in_specs=[whole] * 7 + [scalar, whole],
-        out_specs=whole,
+        in_specs=[hbm] * 9,
+        out_specs=hbm,
+        scratch_shapes=[
+            pltpu.VMEM((seqs * span, depth), BF16),
+            pltpu.VMEM((seqs, depth), BF16),
+            pltpu.VMEM((depth, HD), BF16),
+            pltpu.VMEM((depth, HD), BF16),
+            pltpu.VMEM((depth, HD), BF16),
+            pltpu.VMEM((2 * heads, depth), BF16),
+            pltpu.SMEM((heads,), F32),
+            pltpu.VMEM((seqs, span), F32),
+            pltpu.VMEM((n_y, 144, HD), BF16),
+            pltpu.SemaphoreType.DMA((9,)),
+            pltpu.SemaphoreType.DMA((seqs + 1,)),
+        ],
         cost_estimate=pl.CostEstimate(
             flops=2 * seqs * span * depth * 3 * HD, bytes_accessed=6 << 20, transcendentals=0
         ),
@@ -307,6 +344,7 @@
         out_shape=jax.ShapeDtypeStruct((n_z, 16, HD), BF16),
         in_specs=[whole],
         out_specs=whole,
+        compiler_params=pltpu.CompilerParams(vmem_limit_bytes=16 << 20),
     )(arrived)
     gathered = lax.all_to_all(group, "sp_0", 0, 0, tiled=True)
 
@@ -320,6 +358,7 @@
         ),
         in_specs=[whole] * 7,
         out_specs=(whole,) * 4,
+        compiler_params=pltpu.CompilerParams(vmem_limit_bytes=16 << 20),
     )(gathered, query, new_key, new_value, new_in, new_forget, w_out)
     parts = lax.all_to_all(partial, "tp", 0, 0, tiled=True)
     read = parts.astype(F32).sum(axis=0).astype(BF16)

time: 85.8 us -> 81 us (0.944)
  Pallas kernels: 11.8 us -> 8.58 us
  local copies, waits for them, and re-layouts: 4.01 us -> 1.29 us
  waiting for transfers between devices: 20.7 us -> 23.1 us
  matrix products: 6.77 us -> 5.64 us
    unnamed x13 -> x9, local copies, waits for them, and re-layouts: 2.74 us -> 0.61 us
    all_to_all x1, waiting for transfers between devices: 7.69 us -> 9.46 us  [per_device(): arrived = lax.all_to_all(sent, 'sp_1', 0, 0, tiled=True)]
    pallas_call x1, Pallas kernels: 2.58 us -> 1.24 us  [per_device(): pl.pallas_call(functools.partial(final_kernel, seqs, n_z, n_tp), out_shap...]
    pallas_call x1, Pallas kernels: 2.11 us -> 1.04 us  [per_device(): pl.pallas_call(functools.partial(group_kernel, seqs, n_y, n_z), out_shape...]
  transfers between devices with their start and end apart: 3 -> 3, of which waited for: 3 -> 3; matrix products, arithmetic and copies ran while one was open for 11% -> 9% of each run, Pallas kernels for 0% -> 0%
where the time goes in v2:
time: 81 us; the launch traced here: 80.4 us
  starting transfers between devices  40.4 us (50%)
  waiting for transfers between devices  23.1 us (29%)
  Pallas kernels  8.58 us (11%)
  matrix products  5.64 us (7%)
  local copies, waits for them, and re-layouts  1.29 us (2%)
    all_to_all x1, starting transfers between devices, per_device(): gathered = lax.all_to_all(group, 'sp_0', 0, 0, tiled=True)  25.1 us
    all_to_all x1, waiting for transfers between devices, per_device(): arrived = lax.all_to_all(sent, 'sp_1', 0, 0, tiled=True)  9.46 us
    all_to_all x1, waiting for transfers between devices, per_device(): gathered = lax.all_to_all(group, 'sp_0', 0, 0, tiled=True)  9.04 us
    all_to_all x1, starting transfers between devices, per_device(): parts = lax.all_to_all(partial, 'tp', 0, 0, tiled=True)  7.66 us
    all_to_all x1, starting transfers between devices, per_device(): arrived = lax.all_to_all(sent, 'sp_1', 0, 0, tiled=True)  7.65 us
    pallas_call x1, Pallas kernels, per_device(): pl.pallas_call(functools.partial(block_kernel, seqs, n_y), out_shape=jax....  6.29 us
    all_to_all x1, waiting for transfers between devices, per_device(): parts = lax.all_to_all(partial, 'tp', 0, 0, tiled=True)  4.65 us
    dot_general x3, matrix products, rounded(): jnp.dot(next_tokens, w, preferred_element_type=F32).astype(BF16).astype(F32)  3.2 us
  transfers between devices with their start and end apart: 3, of which 3 were waited for; matrix products, arithmetic and copies ran while one was open for 9% of the time, Pallas kernels for 0%

profile of v2, /device:TPU:1, one launch (start us, length us, event | category | flops | bytes accessed | tf_op | source)
XLA Modules:
  0.0 80.4 jit_solution(1746339633492391404)
XLA Ops:
  0.6 0.0 copy-start.3
  0.6 0.0 copy-start.2
  0.7 0.0 copy-start.1
  0.7 6.3 %shard_map.129 = bf16[8,144,256]{2,1,0:T(8,128)(2,1)} custom-call(bf16[512,2048]{1,0:T(8,128)(2,1)} %bitcast.30, bf16[4,2048]{1,0:T(4,128)(2,1)} %next_hbm.1, bf16[2048,256]{1,0:T(8,128)(2,1)} %w_query_hbm.1, bf16[2048,256]{1,0:T(8,128)(2,1)} %w_key_hbm.1, bf16[2048,256]{1,0:T(8,128)(2,1)} %w_value_hbm.1, bf16[8,2048]{1,0:T(8,128)(2,1)} %bitcast.32, ...), custom_call_target="tpu_custom_call" | custom-call | flops 1610612736 | bytes 6291456 | tf_op jit(solution)/shard_map/pallas_call | solution.py:292
  7.0 7.7 %all-to-all-start = ((bf16[8,144,256]{2,1,0:T(8,128)(2,1)}), bf16[8,144,256]{2,1,0:T(8,128)(2,1)S(1)}, u32[]{:S(2)}, u32[]{:S(2)}) async-start(bf16[8,144,256]{2,1,0:T(8,128)(2,1)} %shard_map.129), calls=%async_computation | async-start | bytes 1179648 | tf_op jit(solution)/shard_map/all_to_all | solution.py:324
  14.6 0.0 copy-done.3
  14.6 0.6 dynamic_slice.11
  15.2 0.0 copy-done.2
  15.2 1.5 %fusion.11 = f32[4,1]{0,1:T(1,128)S(1)} fusion(bf16[4,2048]{1,0:T(4,128)(2,1)S(1)} %copy-done.2, bf16[2048,8]{0,1:T(8,128)(2,1)} %param.16, s32[]{:T(128)S(6)} %select_n.11, f32[]{:T(128)} %bitcast.7), kind=kOutput, calls=%fused_computation.15 | convolution fusion | flops 16420 | bytes 25108 | tf_op jit(solution)/shard_map/dot_general | solution.py:339
  16.8 0.1 copy.15.new_forget_ref
  16.9 0.9 %convolution_bitcast_fusion.new_in_ref = f32[4,1]{1,0:T(4,128)S(1)} fusion(bf16[4,2048]{1,0:T(4,128)(2,1)S(1)} %copy-done.2, bf16[2048,8]{0,1:T(8,128)(2,1)} %param.15, s32[]{:T(128)S(6)} %select_n.11), kind=kOutput, calls=%fused_computation.7 | convolution fusion | flops 16384 | bytes 24596 | tf_op jit(solution)/shard_map/dot_general | solution.py:337
  17.7 0.0 copy-done.1
  17.7 0.0 copy-start
  17.8 0.2 fusion.3.query_ref
  18.0 9.5 %all-to-all-done.in_ref = bf16[8,144,256]{2,1,0:T(8,128)(2,1)S(1)} async-done(((bf16[8,144,256]{2,1,0:T(8,128)(2,1)}), bf16[8,144,256]{2,1,0:T(8,128)(2,1)S(1)}, u32[]{:S(2)}, u32[]{:S(2)}) %all-to-all-start) | async-done | bytes 589856 | tf_op jit(solution)/shard_map/all_to_all | solution.py:324
  27.5 1.0 %shard_map.130 = bf16[16,16,256]{2,1,0:T(8,128)(2,1)} custom-call(bf16[8,144,256]{2,1,0:T(8,128)(2,1)S(1)} %all-to-all-done.in_ref), custom_call_target="tpu_custom_call" | custom-call | tf_op jit(solution)/shard_map/pallas_call | solution.py:342
  28.5 25.1 %all-to-all-start.1 = ((bf16[16,16,256]{2,1,0:T(8,128)(2,1)}), bf16[16,16,256]{2,1,0:T(8,128)(2,1)S(1)}, u32[]{:S(2)}, u32[]{:S(2)}) async-start(bf16[16,16,256]{2,1,0:T(8,128)(2,1)} %shard_map.130), calls=%async_computation.1 | async-start | bytes 262144 | tf_op jit(solution)/shard_map/all_to_all | solution.py:349
  53.6 1.5 %fusion.2.key_ref = f32[4,256]{1,0:T(4,128)S(1)} fusion(bf16[4,2048]{1,0:T(4,128)(2,1)S(1)} %copy-done.2, bf16[2048,256]{1,0:T(8,128)(2,1)} %w_key_hbm.1), kind=kOutput, calls=%fused_computation.4 | convolution fusion | flops 4197376 | bytes 1069056 | tf_op jit(solution)/shard_map/dot_general | solution.py:332
  55.1 1.5 %fusion.value_ref = f32[4,256]{1,0:T(4,128)S(1)} fusion(bf16[4,2048]{1,0:T(4,128)(2,1)S(1)} %copy-done.2, bf16[2048,256]{1,0:T(8,128)(2,1)} %w_value_hbm.1), kind=kOutput, calls=%fused_computation.1 | convolution fusion | flops 4196352 | bytes 1069056 | tf_op jit(solution)/shard_map/dot_general | solution.py:332
  56.6 9.0 %all-to-all-done.1.in_ref = bf16[16,16,256]{2,1,0:T(8,128)(2,1)S(1)} async-done(((bf16[16,16,256]{2,1,0:T(8,128)(2,1)}), bf16[16,16,256]{2,1,0:T(8,128)(2,1)S(1)}, u32[]{:S(2)}, u32[]{:S(2)}) %all-to-all-start.1) | async-done | bytes 131104 | tf_op jit(solution)/shard_map/all_to_all | solution.py:349
  65.6 0.0 copy-done
  65.6 1.2 %shard_map.131 = (bf16[8,256]{1,0:T(8,128)(2,1)}, f32[1,8]{1,0:T(1,128)}, f32[4,1]{1,0:T(4,128)S(1)}, bf16[8,4,2048]{2,1,0:T(4,128)(2,1)}) custom-call(bf16[16,16,256]{2,1,0:T(8,128)(2,1)S(1)} %all-to-all-done.1.in_ref, f32[4,256]{1,0:T(4,128)S(1)} %fusion.3.query_ref, f32[4,256]{1,0:T(4,128)S(1)} %fusion.2.key_ref, f32[4,256]{1,0:T(4,128)S(1)} %fusion.value_ref, ...), custom_call_target="tpu_custom_call" | custom-call | tf_op jit(solution)/shard_map/pallas_call | solution.py:351
  66.9 7.7 %all-to-all-start.2 = ((bf16[8,4,2048]{2,1,0:T(4,128)(2,1)}), bf16[8,4,2048]{2,1,0:T(4,128)(2,1)S(1)}, u32[]{:S(2)}, u32[]{:S(2)}) async-start(bf16[8,4,2048]{2,1,0:T(4,128)(2,1)} %get-tuple-element.11), calls=%async_computation.2 | async-start | bytes 262144 | tf_op jit(solution)/shard_map/all_to_all | solution.py:363
  74.5 0.6 copy.16
  75.1 4.6 %all-to-all-done.2 = bf16[8,4,2048]{2,1,0:T(4,128)(2,1)S(1)} async-done(((bf16[8,4,2048]{2,1,0:T(4,128)(2,1)}), bf16[8,4,2048]{2,1,0:T(4,128)(2,1)S(1)}, u32[]{:S(2)}, u32[]{:S(2)}) %all-to-all-start.2) | async-done | bytes 131104 | tf_op jit(solution)/shard_map/all_to_all | solution.py:363
  79.8 0.7 reduce_sum.12
Async XLA Ops:
  0.6 14.0 %copy-start.3 = (f32[8]{0:T(128)S(1)}, f32[8]{0:T(128)}, u32[]{:S(2)}) copy-start(f32[8]{0:T(128)} %bias_hbm.1) | copy-start | bytes 100
  0.6 14.6 %copy-start.2 = (bf16[4,2048]{1,0:T(4,128)(2,1)S(1)}, bf16[4,2048]{1,0:T(4,128)(2,1)}, u32[]{:S(2)}) copy-start(bf16[4,2048]{1,0:T(4,128)(2,1)} %next_hbm.1) | copy-start | bytes 49156
  0.7 17.1 %copy-start.1 = (bf16[2048,256]{1,0:T(8,128)(2,1)S(1)}, bf16[2048,256]{1,0:T(8,128)(2,1)}, u32[]{:S(2)}) copy-start(bf16[2048,256]{1,0:T(8,128)(2,1)} %w_query_hbm.1) | copy-start | bytes 3145732
  7.0 20.5 %all-to-all-start = ((bf16[8,144,256]{2,1,0:T(8,128)(2,1)}), bf16[8,144,256]{2,1,0:T(8,128)(2,1)S(1)}, u32[]{:S(2)}, u32[]{:S(2)}) async-start(bf16[8,144,256]{2,1,0:T(8,128)(2,1)} %shard_map.129), calls=%async_computation | async-start | bytes 1179648 | tf_op jit(solution)/shard_map/all_to_all | solution.py:324
  17.7 47.9 %copy-start = (bf16[256,2048]{1,0:T(8,128)(2,1)S(1)}, bf16[256,2048]{1,0:T(8,128)(2,1)}, u32[]{:S(2)}) copy-start(bf16[256,2048]{1,0:T(8,128)(2,1)} %w_out_ref.1) | copy-start | bytes 3145732
  28.5 37.1 %all-to-all-start.1 = ((bf16[16,16,256]{2,1,0:T(8,128)(2,1)}), bf16[16,16,256]{2,1,0:T(8,128)(2,1)S(1)}, u32[]{:S(2)}, u32[]{:S(2)}) async-start(bf16[16,16,256]{2,1,0:T(8,128)(2,1)} %shard_map.130), calls=%async_computation.1 | async-start | bytes 262144 | tf_op jit(solution)/shard_map/all_to_all | solution.py:349
  66.9 12.9 %all-to-all-start.2 = ((bf16[8,4,2048]{2,1,0:T(4,128)(2,1)}), bf16[8,4,2048]{2,1,0:T(4,128)(2,1)S(1)}, u32[]{:S(2)}, u32[]{:S(2)}) async-start(bf16[8,4,2048]{2,1,0:T(4,128)(2,1)} %get-tuple-element.11), calls=%async_computation.2 | async-start | bytes 262144 | tf_op jit(solution)/shard_map/all_to_all | solution.py:363

commit v3 on v2

v3 whole, which is shorter than its diff:
```python
import functools

import jax
import jax.numpy as jnp
from jax import lax
from jax.experimental import pallas as pl
from jax.experimental.pallas import tpu as pltpu
from jax.sharding import Mesh
from jax.sharding import PartitionSpec as P

HD = 256
SP = ("sp_0", "sp_1")
LANES = 128
F32 = jnp.float32
BF16 = jnp.bfloat16

NT = (((1,), (1,)), ((), ()))
TN = (((0,), (0,)), ((), ()))


def parts3(x):
    hi = x.astype(BF16).astype(F32)
    rest = x - hi
    mid = rest.astype(BF16).astype(F32)
    return hi, mid, rest - mid


def log_sigmoid(x):
    return jnp.minimum(x, 0.0) - jnp.log1p(jnp.exp(-jnp.abs(x)))


def lanes_of(shape):
    return lax.broadcasted_iota(jnp.int32, shape, len(shape) - 1)


def stats_from(rows):
    return rows, pltpu.roll(rows, LANES - 4, 1), pltpu.roll(rows, LANES - 8, 1)


def later_sums(total):
    later = [jnp.zeros_like(total[:1])]
    for i in range(total.shape[0] - 1, 0, -1):
        later.append(later[-1] + total[i : i + 1])
    later.reverse()
    return later


def norm_halves(norm):
    left, right = norm[:, :LANES], norm[:, LANES:]
    at = lanes_of(left.shape)

    def joined(a, b, c, d):
        turned = [
            pltpu.roll(v, shift, 1) if shift else v
            for v, shift in zip((left, left, right, right), (a, b, c, d), strict=True)
        ]
        low = jnp.where(at < 32, turned[0], turned[1])
        return jnp.where(at < 64, low, jnp.where(at < 96, turned[2], turned[3]))

    return joined(0, 96, 64, 32), joined(96, 64, 32, 0)


def block_kernel(
    seqs,
    n_y,
    tokens_hbm,
    next_hbm,
    w_query_hbm,
    w_key_hbm,
    w_value_hbm,
    in_gate_hbm,
    forget_gate_hbm,
    bias_hbm,
    decay_hbm,
    out_hbm,
    next_out_hbm,
    tokens_ref,
    next_ref,
    w_query_ref,
    w_key_ref,
    w_value_ref,
    gate_ref,
    bias_ref,
    decay_ref,
    out_ref,
    next_out_ref,
    sems,
    out_sems,
):
    head = lax.axis_index("tp")
    count, depth = tokens_hbm.shape
    heads = in_gate_hbm.shape[0]
    span = count // seqs
    scale = HD ** (-0.5)
    moves = [
        (in_gate_hbm, gate_ref.at[pl.ds(0, heads)]),
        (forget_gate_hbm, gate_ref.at[pl.ds(heads, heads)]),
        (tokens_hbm, tokens_ref.at[pl.ds(0, count)]),
        (bias_hbm, bias_ref),
        (decay_hbm, decay_ref),
        (w_key_hbm, w_key_ref),
        (next_hbm, next_ref),
        (w_query_hbm, w_query_ref),
        (w_value_hbm, w_value_ref),
    ]
    copies = [pltpu.make_async_copy(a, b, sems.at[i]) for i, (a, b) in enumerate(moves)]
    for copy in copies:
        copy.start()
    after = (
        lax.broadcasted_iota(jnp.int32, (span, span), 0)
        > lax.broadcasted_iota(jnp.int32, (span, span), 1)
    ).astype(BF16)
    for copy in copies:
        copy.wait()
    following = next_ref[...]
    tokens_ref[count:, :] = jnp.concatenate(
        [following.astype(F32), jnp.zeros((16 - seqs, depth), F32)], axis=0
    ).astype(BF16)

    gates = lax.dot_general(gate_ref[...], tokens_ref[...], NT, preferred_element_type=F32)
    row = lax.broadcasted_iota(jnp.int32, gates.shape, 0)
    log_in = jnp.sum(jnp.where(row == head, gates, 0.0), axis=0, keepdims=True)
    forget = jnp.sum(jnp.where(row == head + heads, gates, 0.0), axis=0, keepdims=True)
    blank = jnp.zeros((1, span - 16), F32)
    new_rows = [jnp.concatenate([v[:, count:], blank], axis=1) for v in (log_in, forget)]
    log_in, forget = (
        jnp.concatenate([v[:, p * span : (p + 1) * span] for p in range(seqs)], axis=0)
        for v in (log_in, forget)
    )
    log_forget = log_sigmoid(forget + bias_ref[head]) + decay_ref[...]
    new_rows[1] = log_sigmoid(new_rows[1] + bias_ref[head])
    split = jnp.concatenate(parts3(log_forget) + (jnp.zeros((seqs, span), F32),), axis=0)
    sums = jnp.dot(split.astype(BF16), after, preferred_element_type=F32)
    suffix = sums[:seqs] + sums[seqs : 2 * seqs] + sums[2 * seqs : 3 * seqs]
    total = jnp.sum(log_forget, axis=1, keepdims=True)
    score = suffix + log_in
    peak = jnp.max(score, axis=1, keepdims=True)
    weight = jnp.exp(score - peak) * scale
    stats = [jnp.broadcast_to(v, (seqs, span)) for v in (total, peak)]
    fill = jnp.zeros((LANES - 3 * seqs - 2, span), F32)
    turned = jnp.transpose(jnp.concatenate([weight] + stats + new_rows + [fill], axis=0))

    keys = jnp.dot(tokens_ref[...], w_key_ref[...], preferred_element_type=F32)
    weighted = []
    for p in range(seqs):
        rows = slice(p * span, (p + 1) * span)
        rounded = keys[rows].astype(BF16).astype(F32)
        weighted.append((rounded * turned[:, p : p + 1]).astype(BF16))
    query = jnp.dot(following, w_query_ref[...], preferred_element_type=F32).astype(BF16)
    new_key = keys[count : count + seqs].astype(BF16).astype(F32) * scale
    query_key = jnp.sum(query.astype(F32) * new_key, axis=1, keepdims=True)

    values = jnp.dot(tokens_ref[...], w_value_ref[...], preferred_element_type=F32).astype(BF16)
    next_out_ref[:seqs, :HD] = values[count : count + seqs].astype(F32)
    wide_at = lanes_of((seqs, LANES))
    new_in, new_forget = (turned[:seqs, 3 * seqs + i : 3 * seqs + i + 1] for i in range(2))
    next_out_ref[:seqs, HD:] = jnp.where(
        wide_at == 0, query_key, jnp.where(wide_at == 1, new_in, new_forget)
    )
    next_send = pltpu.make_async_copy(
        next_out_ref, next_out_hbm.at[pl.ds(0, 8)], out_sems.at[seqs + 1]
    )
    next_send.start()
    at = lanes_of((1, LANES))
    stats = jnp.where(at < seqs, 0.0, turned[:1])
    ones = jnp.ones((8, span), BF16)
    reads_of, norms, sends = [], [], []

    def send(start, size):
        part = pl.ds(start, size)
        sends.append(
            pltpu.make_async_copy(
                out_ref.at[:, part, :], out_hbm.at[:, part, :], out_sems.at[len(sends)]
            )
        )
        sends[-1].start()

    run = HD // 4
    for p in range(seqs):
        rows = slice(p * span, (p + 1) * span)
        memory = lax.dot_general(weighted[p], values[rows], TN, preferred_element_type=F32)
        for y in range(n_y):
            pieces = [memory[r * run + y * 8 : r * run + y * 8 + 8] for r in range(4)]
            out_ref[y, p * 32 : (p + 1) * 32, :] = jnp.concatenate(pieces, axis=0).astype(BF16)
        send(p * 32, 32)
        norms.append(jnp.dot(ones, weighted[p], preferred_element_type=F32)[:1])
        along = lax.dot_general(query, weighted[p], NT, preferred_element_type=F32)[p : p + 1]
        stats = jnp.where(at == p, jnp.sum(along, axis=1, keepdims=True), stats)
        stacked = jnp.concatenate(parts3(along) + (jnp.zeros((5, span), F32),), axis=0)
        reads = jnp.dot(stacked.astype(BF16), values[rows], preferred_element_type=F32)
        reads_of.append(jnp.sum(reads, axis=0, keepdims=True))
    stats = jnp.concatenate(parts3(stats) + (jnp.zeros((1, LANES), F32),), axis=0)
    halves = norm_halves(jnp.concatenate(norms + [jnp.zeros((8 - seqs, HD), F32)], axis=0))
    for i, half in enumerate(halves):
        wide = jnp.concatenate([stats, half[:seqs]], axis=1)
        extra = jnp.concatenate(reads_of + [wide], axis=0).astype(BF16)
        for y in range(i * n_y // 2, (i + 1) * n_y // 2):
            out_ref[y, 128:136, :] = extra
    send(128, 8)
    for copy in sends + [next_send]:
        copy.wait()


def group_kernel(seqs, n_y, n_z, in_ref, out_ref):
    extras = [in_ref[y, 128:136, :].astype(F32) for y in range(n_y)]
    rows = jnp.concatenate(
        [e[4:5, :LANES] + e[5:6, :LANES] + e[6:7, :LANES] for e in extras], axis=0
    )
    query_norm, total, peak = stats_from(rows)
    later = later_sums(total)
    scores = [later[y] + peak[y : y + 1] for y in range(n_y)]
    group_total = later[0] + total[:1]
    group_peak = functools.reduce(jnp.maximum, scores)
    coef = jnp.exp(jnp.concatenate(scores, axis=0) - group_peak)
    group_norm = jnp.sum(coef * query_norm, axis=0, keepdims=True)
    tall = jnp.transpose(jnp.concatenate([coef] * (LANES // n_y), axis=0))
    per_y = [jnp.broadcast_to(tall[:8, y : y + 1], (8, HD)) for y in range(n_y)]

    at = lanes_of((1, LANES))
    total_there = pltpu.roll(jnp.broadcast_to(group_total, (8, LANES)), 4, 1)[:1]
    peak_there = pltpu.roll(jnp.broadcast_to(group_peak, (8, LANES)), 8, 1)[:1]
    packed = jnp.where(at < 4, group_norm, jnp.where(at < 8, total_there, peak_there))
    stats = jnp.concatenate(parts3(jnp.where(at < 12, packed, 0.0)), axis=0)
    reads = jnp.zeros((seqs, HD), F32)
    norms = jnp.zeros((seqs, LANES), F32)
    for y in range(n_y):
        reads += per_y[y][:seqs] * extras[y][:seqs]
        norms += per_y[y][:seqs, :LANES] * extras[y][seqs : 2 * seqs, LANES:]
    for p in range(seqs):
        memory = jnp.zeros((32, HD), F32)
        for y in range(n_y):
            memory += per_y[y][p : p + 1] * in_ref[y, p * 32 : (p + 1) * 32, :].astype(F32)
        side = jnp.concatenate([norms[p : p + 1], jnp.zeros((2, LANES), F32)], axis=0)
        tail = jnp.concatenate(
            [reads, jnp.concatenate([stats, side], axis=1), jnp.zeros((1, HD), F32)], axis=0
        )
        for r in range(n_z // seqs):
            block = jnp.concatenate([memory[r * 8 : r * 8 + 8], tail], axis=0)
            out_ref[p * (n_z // seqs) + r] = block.astype(BF16)


def final_kernel(
    seqs, n_z, n_tp, in_ref, next_ref, w_out_ref, memory_ref, norm_ref, stab_ref, head_ref
):
    z = lax.axis_index("sp_0")
    y = lax.axis_index("sp_1")
    per_prompt = n_z // seqs
    mine = z // per_prompt
    blocks = [in_ref[i].astype(F32) for i in range(n_z)]
    rows = jnp.concatenate(
        [b[12:13, :LANES] + b[13:14, :LANES] + b[14:15, :LANES] for b in blocks], axis=0
    )
    query_norm, total, peak = stats_from(rows)
    later = later_sums(total)
    scores = [later[i] + peak[i : i + 1] for i in range(n_z)]
    stab = functools.reduce(jnp.maximum, scores, later[0] + total[:1])
    coef = jnp.exp(jnp.concatenate(scores, axis=0) - stab)
    all_norm = jnp.sum(coef * query_norm, axis=0, keepdims=True)
    filled = jnp.zeros((LANES - n_z - 2, LANES), F32)
    tall = jnp.transpose(jnp.concatenate([coef, stab, all_norm, filled], axis=0))[:8]
    stab4 = tall[:seqs, n_z : n_z + 1]
    query_norm4 = tall[:seqs, n_z + 1 : n_z + 2]
    stab_ref[...] = stab[:, :seqs]

    query_state = jnp.zeros((seqs, HD), F32)
    for i in range(n_z):
        query_state += tall[:seqs, i : i + 1] * blocks[i][8:12]
    new_value = next_ref[:seqs, :HD]
    query_key, new_in, new_forget = (next_ref[:seqs, HD + i : HD + i + 1] for i in range(3))
    carried = new_forget + stab4
    top = jnp.maximum(carried, new_in)
    keep = jnp.exp(carried - top)
    take = jnp.exp(new_in - top)
    numer = keep * query_state + take * query_key * new_value
    denom = keep * query_norm4 + take * query_key
    head_out = (numer / jnp.maximum(jnp.abs(denom), 1.0)).astype(BF16)
    partial = jnp.dot(head_out, w_out_ref[...], preferred_element_type=F32).astype(BF16)
    for i in range(n_tp):
        head_ref[i] = partial

    is_mine = lanes_of(coef.shape) == mine
    own = jnp.sum(jnp.where(is_mine, coef, 0.0), axis=1, keepdims=True)
    memory = jnp.zeros((8, HD), F32)
    norm = jnp.zeros((1, LANES), F32)
    for i in range(n_z):
        memory += own[i : i + 1] * blocks[i][:8]
        norm += own[i : i + 1] * blocks[i][12:13, LANES:]
    memory_ref[...] = memory.astype(BF16)
    first = lax.rem(z, per_prompt) * 32 + lax.rem(y, 4) * 8
    turned = pltpu.roll(jnp.broadcast_to(norm, (8, LANES)), lax.rem(LANES - first, LANES), 1)
    norm_ref[...] = turned[:1, :8]


def sum_kernel(in_ref, out_ref):
    parts = in_ref[...].astype(F32)
    out_ref[...] = jnp.sum(parts, axis=0).astype(BF16)


def per_device(
    tokens,
    next_tokens,
    w_query,
    w_key,
    w_value,
    w_in_gate,
    w_forget_gate,
    forget_bias,
    extra_decay,
    w_out,
):
    seqs, span, depth = tokens.shape
    heads = w_in_gate.shape[1]
    n_z, n_y, n_tp = (lax.axis_size(a) for a in ("sp_0", "sp_1", "tp"))
    vmem = pl.BlockSpec(memory_space=pltpu.VMEM)
    hbm = pl.BlockSpec(memory_space=pltpu.HBM)
    limit = pltpu.CompilerParams(vmem_limit_bytes=16 << 20)

    sent, following = pl.pallas_call(
        functools.partial(block_kernel, seqs, n_y),
        out_shape=(
            jax.ShapeDtypeStruct((n_y, 136, HD), BF16),
            jax.ShapeDtypeStruct((64, HD + LANES), F32),
        ),
        in_specs=[hbm] * 9,
        out_specs=(hbm, hbm),
        scratch_shapes=[
            pltpu.VMEM((seqs * span + 16, depth), BF16),
            pltpu.VMEM((seqs, depth), BF16),
            pltpu.VMEM((depth, HD), BF16),
            pltpu.VMEM((depth, HD), BF16),
            pltpu.VMEM((depth, HD), BF16),
            pltpu.VMEM((2 * heads, depth), BF16),
            pltpu.SMEM((heads,), F32),
            pltpu.VMEM((seqs, span), F32),
            pltpu.VMEM((n_y, 136, HD), BF16),
            pltpu.VMEM((8, HD + LANES), F32),
            pltpu.SemaphoreType.DMA((9,)),
            pltpu.SemaphoreType.DMA((seqs + 2,)),
        ],
    )(
        tokens.reshape(seqs * span, depth),
        next_tokens,
        w_query,
        w_key,
        w_value,
        w_in_gate.T,
        w_forget_gate.T,
        forget_bias,
        extra_decay.reshape(seqs, span),
    )
    arrived = lax.all_to_all(sent, "sp_1", 0, 0, tiled=True)
    group = pl.pallas_call(
        functools.partial(group_kernel, seqs, n_y, n_z),
        out_shape=jax.ShapeDtypeStruct((n_z, 16, HD), BF16),
        in_specs=[vmem],
        out_specs=vmem,
        compiler_params=limit,
    )(arrived)
    gathered = lax.all_to_all(group, "sp_0", 0, 0, tiled=True)
    memory, norm, stab, partial = pl.pallas_call(
        functools.partial(final_kernel, seqs, n_z, n_tp),
        out_shape=(
            jax.ShapeDtypeStruct((8, HD), BF16),
            jax.ShapeDtypeStruct((1, 8), F32),
            jax.ShapeDtypeStruct((1, seqs), F32),
            jax.ShapeDtypeStruct((n_tp, seqs, depth), BF16),
        ),
        in_specs=[vmem] * 3,
        out_specs=(vmem,) * 4,
        compiler_params=limit,
    )(gathered, following, w_out)
    parts = lax.all_to_all(partial, "tp", 0, 0, tiled=True)
    read = pl.pallas_call(
        sum_kernel,
        out_shape=jax.ShapeDtypeStruct((seqs, depth), BF16),
        in_specs=[vmem],
        out_specs=vmem,
        compiler_params=limit,
    )(parts)
    return memory[None], norm, stab.reshape(seqs, 1), read


def solution(mesh):
    torus = Mesh(mesh.devices.reshape(16, 8, mesh.shape["tp"]), ("sp_0", "sp_1", "tp"))
    placed = (
        P(None, SP, None),
        P(),
        P(None, "tp"),
        P(None, "tp"),
        P(None, "tp"),
        P(),
        P(),
        P(),
        P("tp", None, SP),
        P("tp", None),
    )
    return jax.shard_map(
        per_device,
        mesh=torus,
        in_specs=placed,
        out_specs=(P("tp", SP, None), P("tp", SP), P(None, "tp"), P()),
        check_vma=False,
    )
```

time: 81 us -> 77.5 us (0.957)
  blocking collectives: 0 us -> 68.2 us
  starting transfers between devices: 40.4 us -> 0 us
  waiting for transfers between devices: 23.1 us -> 0 us
  matrix products: 5.64 us -> 0 us
  local copies, waits for them, and re-layouts: 1.29 us -> 0.01 us
    all_to_all x0 -> x3, blocking collectives: none -> 68.2 us  [the longest x1 34.6 us: per_device(): gathered = lax.all_to_all(group, 'sp_0', 0, 0, tiled=True)]
    all_to_all x3 -> x0, starting transfers between devices: 40.4 us -> none  [the longest x1 25.1 us: per_device(): gathered = lax.all_to_all(group, 'sp_0', 0, 0, tiled=True)]
    all_to_all x3 -> x0, waiting for transfers between devices: 23.1 us -> none  [the longest x1 9.46 us: per_device(): arrived = lax.all_to_all(sent, 'sp_1', 0, 0, tiled=True)]
    dot_general x5 -> x0, matrix products: 5.64 us -> none  [the longest x3 3.2 us: rounded(): jnp.dot(next_tokens, w, preferred_element_type=F32).astype(BF16).astype(F32)]
    pallas_call x1 -> x2, Pallas kernels: 6.29 us -> 6.81 us  [the longest x1 6.15 us: per_device(): pl.pallas_call(functools.partial(block_kernel, seqs, n_y), out_shape=(jax...]
  transfers between devices with their start and end apart: 3 -> 0, of which waited for: 3 -> 0; matrix products, arithmetic and copies ran while one was open for 9% -> 0% of each run, Pallas kernels for 0% -> 0%
where the time goes in v3:
time: 77.5 us; the launch traced here: 77.2 us
  blocking collectives  68.2 us (88%)
  Pallas kernels  8.33 us (11%)
    all_to_all x1, blocking collectives, per_device(): gathered = lax.all_to_all(group, 'sp_0', 0, 0, tiled=True)  34.6 us
    all_to_all x1, blocking collectives, per_device(): arrived = lax.all_to_all(sent, 'sp_1', 0, 0, tiled=True)  20.3 us
    all_to_all x1, blocking collectives, per_device(): parts = lax.all_to_all(partial, 'tp', 0, 0, tiled=True)  13.3 us
    pallas_call x1, Pallas kernels, per_device(): pl.pallas_call(functools.partial(block_kernel, seqs, n_y), out_shape=(jax...  6.15 us

profile of v3, /device:TPU:1, one launch (start us, length us, event | category | flops | bytes accessed | tf_op | source)
XLA Modules:
  0.0 77.2 jit_solution(679640613638066401)
XLA Ops:
  0.6 6.1 %shard_map.129 = (bf16[8,136,256]{2,1,0:T(8,128)(2,1)}, f32[64,384]{1,0:T(8,128)}) custom-call(bf16[512,2048]{1,0:T(8,128)(2,1)} %bitcast.6, bf16[4,2048]{1,0:T(4,128)(2,1)} %next_hbm.1, bf16[2048,256]{1,0:T(8,128)(2,1)} %w_query_hbm.1, bf16[2048,256]{1,0:T(8,128)(2,1)} %w_key_hbm.1, bf16[2048,256]{1,0:T(8,128)(2,1)} %w_value_hbm.1, ...), custom_call_target="tpu_custom_call" | custom-call | tf_op jit(solution)/shard_map/pallas_call | solution.py:318
  6.8 0.0 copy-start
  6.8 0.0 copy-start.1
  6.8 20.3 %all_to_all.15.in_ref = bf16[8,136,256]{2,1,0:T(8,128)(2,1)S(1)} all-to-all(bf16[8,136,256]{2,1,0:T(8,128)(2,1)} %get-tuple-element.10), channel_id=1, replica_groups=mesh['sp_0'=16,'sp_1'=8,'tp'=8] {'sp_1'}, dimensions={0} | all-to-all | bytes 1114112 | tf_op jit(solution)/shard_map/all_to_all | solution.py:351
  27.1 0.4 shard_map.130
  27.5 34.6 %all_to_all.16.in_ref = bf16[16,16,256]{2,1,0:T(8,128)(2,1)S(1)} all-to-all(bf16[16,16,256]{2,1,0:T(8,128)(2,1)S(1)} %shard_map.130), channel_id=1, replica_groups=mesh['sp_0'=16,'sp_1'=8,'tp'=8] {'sp_0'}, dimensions={0} | all-to-all | bytes 262144 | tf_op jit(solution)/shard_map/all_to_all | solution.py:359
  62.1 0.0 copy-done
  62.1 0.0 copy-done.1
  62.1 1.1 %shard_map.131 = (bf16[8,256]{1,0:T(8,128)(2,1)}, f32[1,8]{1,0:T(1,128)}, f32[1,4]{1,0:T(1,128)}, bf16[8,4,2048]{2,1,0:T(4,128)(2,1)S(1)}) custom-call(bf16[16,16,256]{2,1,0:T(8,128)(2,1)S(1)} %all_to_all.16.in_ref, f32[64,384]{1,0:T(8,128)S(1)} %copy-done.1, bf16[256,2048]{1,0:T(8,128)(2,1)S(1)} %copy-done), custom_call_target="tpu_custom_call" | custom-call | tf_op jit(solution)/shard_map/pallas_call | solution.py:360
  63.2 13.3 %all_to_all.17.in_ref = bf16[8,4,2048]{2,1,0:T(4,128)(2,1)S(1)} all-to-all(bf16[8,4,2048]{2,1,0:T(4,128)(2,1)S(1)} %get-tuple-element.15), channel_id=1, replica_groups=mesh['sp_0'=16,'sp_1'=8,'tp'=8] {'tp'}, dimensions={0} | all-to-all | bytes 262144 | tf_op jit(solution)/shard_map/all_to_all | solution.py:372
  76.5 0.7 shard_map.132
Async XLA Ops:
  6.8 55.3 %copy-start = (bf16[256,2048]{1,0:T(8,128)(2,1)S(1)}, bf16[256,2048]{1,0:T(8,128)(2,1)}, u32[]{:S(2)}) copy-start(bf16[256,2048]{1,0:T(8,128)(2,1)} %w_out_ref.1) | copy-start | bytes 3145732
  6.8 55.3 %copy-start.1 = (f32[64,384]{1,0:T(8,128)S(1)}, f32[64,384]{1,0:T(8,128)}, u32[]{:S(2)}) copy-start(f32[64,384]{1,0:T(8,128)} %get-tuple-element.11.next_ref) | copy-start | bytes 294916

commit v4 on v3

--- a/solution.py
+++ b/solution.py
@@ -93,13 +93,13 @@
     span = count // seqs
     scale = HD ** (-0.5)
     moves = [
+        (next_hbm, next_ref),
         (in_gate_hbm, gate_ref.at[pl.ds(0, heads)]),
         (forget_gate_hbm, gate_ref.at[pl.ds(heads, heads)]),
         (tokens_hbm, tokens_ref.at[pl.ds(0, count)]),
         (bias_hbm, bias_ref),
         (decay_hbm, decay_ref),
         (w_key_hbm, w_key_ref),
-        (next_hbm, next_ref),
         (w_query_hbm, w_query_ref),
         (w_value_hbm, w_value_ref),
     ]
@@ -110,7 +110,7 @@
         lax.broadcasted_iota(jnp.int32, (span, span), 0)
         > lax.broadcasted_iota(jnp.int32, (span, span), 1)
     ).astype(BF16)
-    for copy in copies:
+    for copy in copies[:6]:
         copy.wait()
     following = next_ref[...]
     tokens_ref[count:, :] = jnp.concatenate(
@@ -140,6 +140,8 @@
     fill = jnp.zeros((LANES - 3 * seqs - 2, span), F32)
     turned = jnp.transpose(jnp.concatenate([weight] + stats + new_rows + [fill], axis=0))
 
+    for copy in copies[6:]:
+        copy.wait()
     keys = jnp.dot(tokens_ref[...], w_key_ref[...], preferred_element_type=F32)
     weighted = []
     for p in range(seqs):
@@ -240,7 +242,7 @@
 
 
 def final_kernel(
-    seqs, n_z, n_tp, in_ref, next_ref, w_out_ref, memory_ref, norm_ref, stab_ref, head_ref
+    seqs, n_z, n_tp, in_ref, next_ref, w_out_ref, memory_ref, rows_ref, head_ref
 ):
     z = lax.axis_index("sp_0")
     y = lax.axis_index("sp_1")
@@ -260,7 +262,6 @@
     tall = jnp.transpose(jnp.concatenate([coef, stab, all_norm, filled], axis=0))[:8]
     stab4 = tall[:seqs, n_z : n_z + 1]
     query_norm4 = tall[:seqs, n_z + 1 : n_z + 2]
-    stab_ref[...] = stab[:, :seqs]
 
     query_state = jnp.zeros((seqs, HD), F32)
     for i in range(n_z):
@@ -288,12 +289,14 @@
     memory_ref[...] = memory.astype(BF16)
     first = lax.rem(z, per_prompt) * 32 + lax.rem(y, 4) * 8
     turned = pltpu.roll(jnp.broadcast_to(norm, (8, LANES)), lax.rem(LANES - first, LANES), 1)
-    norm_ref[...] = turned[:1, :8]
-
-
-def sum_kernel(in_ref, out_ref):
-    parts = in_ref[...].astype(F32)
-    out_ref[...] = jnp.sum(parts, axis=0).astype(BF16)
+    rows_ref[...] = jnp.concatenate([stab, turned[:7]], axis=0)
+
+
+def last_kernel(seqs, in_ref, memory_in_ref, rows_ref, memory_ref, norm_ref, stab_ref, read_ref):
+    memory_ref[...] = memory_in_ref[...]
+    stab_ref[...] = rows_ref[:1, :seqs]
+    norm_ref[...] = rows_ref[1:2, :8]
+    read_ref[...] = jnp.sum(in_ref[...].astype(F32), axis=0).astype(BF16)
 
 
 def per_device(
@@ -357,26 +360,30 @@
         compiler_params=limit,
     )(arrived)
     gathered = lax.all_to_all(group, "sp_0", 0, 0, tiled=True)
-    memory, norm, stab, partial = pl.pallas_call(
+    memory_here, rows_here, partial = pl.pallas_call(
         functools.partial(final_kernel, seqs, n_z, n_tp),
+        out_shape=(
+            jax.ShapeDtypeStruct((8, HD), BF16),
+            jax.ShapeDtypeStruct((8, LANES), F32),
+            jax.ShapeDtypeStruct((n_tp, seqs, depth), BF16),
+        ),
+        in_specs=[vmem] * 3,
+        out_specs=(vmem,) * 3,
+        compiler_params=limit,
+    )(gathered, following, w_out)
+    parts = lax.all_to_all(partial, "tp", 0, 0, tiled=True)
+    memory, norm, stab, read = pl.pallas_call(
+        functools.partial(last_kernel, seqs),
         out_shape=(
             jax.ShapeDtypeStruct((8, HD), BF16),
             jax.ShapeDtypeStruct((1, 8), F32),
             jax.ShapeDtypeStruct((1, seqs), F32),
-            jax.ShapeDtypeStruct((n_tp, seqs, depth), BF16),
+            jax.ShapeDtypeStruct((seqs, depth), BF16),
         ),
         in_specs=[vmem] * 3,
         out_specs=(vmem,) * 4,
         compiler_params=limit,
-    )(gathered, following, w_out)
-    parts = lax.all_to_all(partial, "tp", 0, 0, tiled=True)
-    read = pl.pallas_call(
-        sum_kernel,
-        out_shape=jax.ShapeDtypeStruct((seqs, depth), BF16),
-        in_specs=[vmem],
-        out_specs=vmem,
-        compiler_params=limit,
-    )(parts)
+    )(parts, memory_here, rows_here)
     return memory[None], norm, stab.reshape(seqs, 1), read
 
 

time: 77.5 us -> 76.6 us (0.988)
  Pallas kernels: 8.33 us -> 7.42 us
where the time goes in v4:
time: 76.6 us; the launch traced here: 76.3 us
  blocking collectives  68.2 us (89%)
  Pallas kernels  7.42 us (10%)
    all_to_all x1, blocking collectives, per_device(): gathered = lax.all_to_all(group, 'sp_0', 0, 0, tiled=True)  34.6 us
    all_to_all x1, blocking collectives, per_device(): arrived = lax.all_to_all(sent, 'sp_1', 0, 0, tiled=True)  20.3 us
    all_to_all x1, blocking collectives, per_device(): parts = lax.all_to_all(partial, 'tp', 0, 0, tiled=True)  13.4 us
    pallas_call x1, Pallas kernels, per_device(): pl.pallas_call(functools.partial(block_kernel, seqs, n_y), out_shape=(jax...  5.66 us

profile of v4, /device:TPU:1, one launch (start us, length us, event | category | flops | bytes accessed | tf_op | source)
XLA Modules:
  0.0 76.3 jit_solution(9496576359436548273)
XLA Ops:
  0.6 5.7 %shard_map.129 = (bf16[8,136,256]{2,1,0:T(8,128)(2,1)}, f32[64,384]{1,0:T(8,128)}) custom-call(bf16[512,2048]{1,0:T(8,128)(2,1)} %bitcast.6, bf16[4,2048]{1,0:T(4,128)(2,1)} %next_hbm.1, bf16[2048,256]{1,0:T(8,128)(2,1)} %w_query_hbm.1, bf16[2048,256]{1,0:T(8,128)(2,1)} %w_key_hbm.1, bf16[2048,256]{1,0:T(8,128)(2,1)} %w_value_hbm.1, ...), custom_call_target="tpu_custom_call" | custom-call | tf_op jit(solution)/shard_map/pallas_call | solution.py:321
  6.3 0.0 copy-start
  6.3 0.0 copy-start.1
  6.3 20.3 %all_to_all.15.in_ref = bf16[8,136,256]{2,1,0:T(8,128)(2,1)S(1)} all-to-all(bf16[8,136,256]{2,1,0:T(8,128)(2,1)} %get-tuple-element.13), channel_id=1, replica_groups=mesh['sp_0'=16,'sp_1'=8,'tp'=8] {'sp_1'}, dimensions={0} | all-to-all | bytes 1114112 | tf_op jit(solution)/shard_map/all_to_all | solution.py:354
  26.6 0.4 shard_map.130
  27.0 34.6 %all_to_all.16.in_ref = bf16[16,16,256]{2,1,0:T(8,128)(2,1)S(1)} all-to-all(bf16[16,16,256]{2,1,0:T(8,128)(2,1)S(1)} %shard_map.130), channel_id=1, replica_groups=mesh['sp_0'=16,'sp_1'=8,'tp'=8] {'sp_0'}, dimensions={0} | all-to-all | bytes 262144 | tf_op jit(solution)/shard_map/all_to_all | solution.py:362
  61.6 0.0 copy-done
  61.6 0.0 copy-done.1
  61.6 0.7 shard_map.131
  62.3 13.4 %all_to_all.17.in_ref = bf16[8,4,2048]{2,1,0:T(4,128)(2,1)S(1)} all-to-all(bf16[8,4,2048]{2,1,0:T(4,128)(2,1)S(1)} %get-tuple-element.15), channel_id=1, replica_groups=mesh['sp_0'=16,'sp_1'=8,'tp'=8] {'tp'}, dimensions={0} | all-to-all | bytes 262144 | tf_op jit(solution)/shard_map/all_to_all | solution.py:374
  75.7 0.7 shard_map.132
Async XLA Ops:
  6.3 55.3 %copy-start = (bf16[256,2048]{1,0:T(8,128)(2,1)S(1)}, bf16[256,2048]{1,0:T(8,128)(2,1)}, u32[]{:S(2)}) copy-start(bf16[256,2048]{1,0:T(8,128)(2,1)} %w_out_ref.1) | copy-start | bytes 3145732
  6.3 55.3 %copy-start.1 = (f32[64,384]{1,0:T(8,128)S(1)}, f32[64,384]{1,0:T(8,128)}, u32[]{:S(2)}) copy-start(f32[64,384]{1,0:T(8,128)} %get-tuple-element.14.next_ref) | copy-start | bytes 294916

commit v5 on v4

--- a/solution.py
+++ b/solution.py
@@ -238,7 +238,7 @@
         )
         for r in range(n_z // seqs):
             block = jnp.concatenate([memory[r * 8 : r * 8 + 8], tail], axis=0)
-            out_ref[p * (n_z // seqs) + r] = block.astype(BF16)
+            out_ref[n_z - 1 - p * (n_z // seqs) - r] = block.astype(BF16)
 
 
 def final_kernel(
@@ -248,7 +248,7 @@
     y = lax.axis_index("sp_1")
     per_prompt = n_z // seqs
     mine = z // per_prompt
-    blocks = [in_ref[i].astype(F32) for i in range(n_z)]
+    blocks = [in_ref[n_z - 1 - i].astype(F32) for i in range(n_z)]
     rows = jnp.concatenate(
         [b[12:13, :LANES] + b[13:14, :LANES] + b[14:15, :LANES] for b in blocks], axis=0
     )
@@ -297,6 +297,11 @@
     stab_ref[...] = rows_ref[:1, :seqs]
     norm_ref[...] = rows_ref[1:2, :8]
     read_ref[...] = jnp.sum(in_ref[...].astype(F32), axis=0).astype(BF16)
+
+
+def exchange_backwards(blocks, axis):
+    backwards = list(range(lax.axis_size(axis)))[::-1]
+    return lax.all_to_all(blocks, axis, 0, 0, tiled=True, axis_index_groups=[backwards])
 
 
 def per_device(
@@ -359,7 +364,7 @@
         out_specs=vmem,
         compiler_params=limit,
     )(arrived)
-    gathered = lax.all_to_all(group, "sp_0", 0, 0, tiled=True)
+    gathered = exchange_backwards(group, "sp_0")
     memory_here, rows_here, partial = pl.pallas_call(
         functools.partial(final_kernel, seqs, n_z, n_tp),
         out_shape=(
@@ -371,7 +376,7 @@
         out_specs=(vmem,) * 3,
         compiler_params=limit,
     )(gathered, following, w_out)
-    parts = lax.all_to_all(partial, "tp", 0, 0, tiled=True)
+    parts = exchange_backwards(partial, "tp")
     memory, norm, stab, read = pl.pallas_call(
         functools.partial(last_kernel, seqs),
         out_shape=(

time: 76.6 us -> 74.8 us (0.977)
  blocking collectives: 68.2 us -> 66.4 us
    all_to_all x2, blocking collectives: 48 us -> 46.1 us  [exchange_backwards(): lax.all_to_all(blocks, axis, 0, 0, tiled=True, axis_index_groups=[backwar...]
where the time goes in v5:
time: 74.8 us; the launch traced here: 74.5 us
  blocking collectives  66.4 us (89%)
  Pallas kernels  7.42 us (10%)
    all_to_all x2, blocking collectives, exchange_backwards(): lax.all_to_all(blocks, axis, 0, 0, tiled=True, axis_index_groups=[backwar...  46.1 us
    all_to_all x1, blocking collectives, per_device(): arrived = lax.all_to_all(sent, 'sp_1', 0, 0, tiled=True)  20.3 us
    pallas_call x1, Pallas kernels, per_device(): pl.pallas_call(functools.partial(block_kernel, seqs, n_y), out_shape=(jax...  5.66 us

profile of v5, /device:TPU:1, one launch (start us, length us, event | category | flops | bytes accessed | tf_op | source)
XLA Modules:
  0.0 74.5 jit_solution(1420974514943043788)
XLA Ops:
  0.6 5.7 %shard_map.129 = (bf16[8,136,256]{2,1,0:T(8,128)(2,1)}, f32[64,384]{1,0:T(8,128)}) custom-call(bf16[512,2048]{1,0:T(8,128)(2,1)} %bitcast.6, bf16[4,2048]{1,0:T(4,128)(2,1)} %next_hbm.1, bf16[2048,256]{1,0:T(8,128)(2,1)} %w_query_hbm.1, bf16[2048,256]{1,0:T(8,128)(2,1)} %w_key_hbm.1, bf16[2048,256]{1,0:T(8,128)(2,1)} %w_value_hbm.1, ...), custom_call_target="tpu_custom_call" | custom-call | tf_op jit(solution)/shard_map/pallas_call | solution.py:326
  6.3 0.0 copy-start
  6.3 0.0 copy-start.1
  6.3 20.3 %all_to_all.15.in_ref = bf16[8,136,256]{2,1,0:T(8,128)(2,1)S(1)} all-to-all(bf16[8,136,256]{2,1,0:T(8,128)(2,1)} %get-tuple-element.13), channel_id=1, replica_groups=mesh['sp_0'=16,'sp_1'=8,'tp'=8] {'sp_1'}, dimensions={0} | all-to-all | bytes 1114112 | tf_op jit(solution)/shard_map/all_to_all | solution.py:359
  26.6 0.4 shard_map.130
  27.0 34.7 %all_to_all.16.in_ref = bf16[16,16,256]{2,1,0:T(8,128)(2,1)S(1)} all-to-all(bf16[16,16,256]{2,1,0:T(8,128)(2,1)S(1)} %shard_map.130), channel_id=1, replica_groups={{960,896,832,768,704,640,576,512,448,384,320,256,192,128,64,0},{961,897..., dimensions={0} | all-to-all | bytes 262144 | tf_op jit(solution)/shard_map/all_to_all | solution.py:304
  61.7 0.0 copy-done
  61.7 0.0 copy-done.1
  61.7 0.7 shard_map.131
  62.4 11.5 %all_to_all.17.in_ref = bf16[8,4,2048]{2,1,0:T(4,128)(2,1)S(1)} all-to-all(bf16[8,4,2048]{2,1,0:T(4,128)(2,1)S(1)} %get-tuple-element.15), channel_id=1, replica_groups={{7,6,5,4,3,2,1,0},{15,14,13,12,11,10,9,8},{23,22,21,20,19,18,17,16},{31..., dimensions={0} | all-to-all | bytes 262144 | tf_op jit(solution)/shard_map/all_to_all | solution.py:304
  73.8 0.7 shard_map.132
Async XLA Ops:
  6.3 55.4 %copy-start = (bf16[256,2048]{1,0:T(8,128)(2,1)S(1)}, bf16[256,2048]{1,0:T(8,128)(2,1)}, u32[]{:S(2)}) copy-start(bf16[256,2048]{1,0:T(8,128)(2,1)} %w_out_ref.1) | copy-start | bytes 3145732
  6.3 55.4 %copy-start.1 = (f32[64,384]{1,0:T(8,128)S(1)}, f32[64,384]{1,0:T(8,128)}, u32[]{:S(2)}) copy-start(f32[64,384]{1,0:T(8,128)} %get-tuple-element.14.next_ref) | copy-start | bytes 294916

commit v6 on v5

--- a/solution.py
+++ b/solution.py
@@ -238,7 +238,7 @@
         )
         for r in range(n_z // seqs):
             block = jnp.concatenate([memory[r * 8 : r * 8 + 8], tail], axis=0)
-            out_ref[n_z - 1 - p * (n_z // seqs) - r] = block.astype(BF16)
+            out_ref[9 * (p * (n_z // seqs) + r) % n_z] = block.astype(BF16)
 
 
 def final_kernel(
@@ -248,7 +248,7 @@
     y = lax.axis_index("sp_1")
     per_prompt = n_z // seqs
     mine = z // per_prompt
-    blocks = [in_ref[n_z - 1 - i].astype(F32) for i in range(n_z)]
+    blocks = [in_ref[9 * i % n_z].astype(F32) for i in range(n_z)]
     rows = jnp.concatenate(
         [b[12:13, :LANES] + b[13:14, :LANES] + b[14:15, :LANES] for b in blocks], axis=0
     )
@@ -364,7 +364,8 @@
         out_specs=vmem,
         compiler_params=limit,
     )(arrived)
-    gathered = exchange_backwards(group, "sp_0")
+    steps = [[9 * i % n_z for i in range(n_z)]]
+    gathered = lax.all_to_all(group, "sp_0", 0, 0, tiled=True, axis_index_groups=steps)
     memory_here, rows_here, partial = pl.pallas_call(
         functools.partial(final_kernel, seqs, n_z, n_tp),
         out_shape=(

time: 74.8 us -> 75.1 us (level)
    all_to_all x0 -> x1, blocking collectives: none -> 34.5 us  [per_device(): lax.all_to_all(group, 'sp_0', 0, 0, tiled=True, axis_index_groups=steps)]
    all_to_all x2 -> x1, blocking collectives: 46.1 us -> 11.9 us  [exchange_backwards(): lax.all_to_all(blocks, axis, 0, 0, tiled=True, axis_index_groups=[backwar...]
where the time goes in v6:
time: 75.1 us; the launch traced here: 74.8 us
  blocking collectives  66.7 us (89%)
  Pallas kernels  7.42 us (10%)
    all_to_all x1, blocking collectives, per_device(): lax.all_to_all(group, 'sp_0', 0, 0, tiled=True, axis_index_groups=steps)  34.5 us
    all_to_all x1, blocking collectives, per_device(): arrived = lax.all_to_all(sent, 'sp_1', 0, 0, tiled=True)  20.3 us
    all_to_all x1, blocking collectives, exchange_backwards(): lax.all_to_all(blocks, axis, 0, 0, tiled=True, axis_index_groups=[backwar...  11.9 us
    pallas_call x1, Pallas kernels, per_device(): pl.pallas_call(functools.partial(block_kernel, seqs, n_y), out_shape=(jax...  5.66 us

profile of v6, /device:TPU:1, one launch (start us, length us, event | category | flops | bytes accessed | tf_op | source)
XLA Modules:
  0.0 74.8 jit_solution(7887665637665179840)
XLA Ops:
  0.6 5.7 %shard_map.129 = (bf16[8,136,256]{2,1,0:T(8,128)(2,1)}, f32[64,384]{1,0:T(8,128)}) custom-call(bf16[512,2048]{1,0:T(8,128)(2,1)} %bitcast.6, bf16[4,2048]{1,0:T(4,128)(2,1)} %next_hbm.1, bf16[2048,256]{1,0:T(8,128)(2,1)} %w_query_hbm.1, bf16[2048,256]{1,0:T(8,128)(2,1)} %w_key_hbm.1, bf16[2048,256]{1,0:T(8,128)(2,1)} %w_value_hbm.1, ...), custom_call_target="tpu_custom_call" | custom-call | tf_op jit(solution)/shard_map/pallas_call | solution.py:326
  6.3 0.0 copy-start
  6.3 0.0 copy-start.1
  6.3 20.3 %all_to_all.15.in_ref = bf16[8,136,256]{2,1,0:T(8,128)(2,1)S(1)} all-to-all(bf16[8,136,256]{2,1,0:T(8,128)(2,1)} %get-tuple-element.13), channel_id=1, replica_groups=mesh['sp_0'=16,'sp_1'=8,'tp'=8] {'sp_1'}, dimensions={0} | all-to-all | bytes 1114112 | tf_op jit(solution)/shard_map/all_to_all | solution.py:359
  26.6 0.4 shard_map.130
  27.0 34.5 %all_to_all.16.in_ref = bf16[16,16,256]{2,1,0:T(8,128)(2,1)S(1)} all-to-all(bf16[16,16,256]{2,1,0:T(8,128)(2,1)S(1)} %shard_map.130), channel_id=1, replica_groups={{0,576,128,704,256,832,384,960,512,64,640,192,768,320,896,448},{1,577,1..., dimensions={0} | all-to-all | bytes 262144 | tf_op jit(solution)/shard_map/all_to_all | solution.py:368
  61.5 0.0 copy-done
  61.5 0.0 copy-done.1
  61.5 0.7 shard_map.131
  62.2 11.9 %all_to_all.17.in_ref = bf16[8,4,2048]{2,1,0:T(4,128)(2,1)S(1)} all-to-all(bf16[8,4,2048]{2,1,0:T(4,128)(2,1)S(1)} %get-tuple-element.15), channel_id=1, replica_groups={{7,6,5,4,3,2,1,0},{15,14,13,12,11,10,9,8},{23,22,21,20,19,18,17,16},{31..., dimensions={0} | all-to-all | bytes 262144 | tf_op jit(solution)/shard_map/all_to_all | solution.py:304
  74.1 0.7 shard_map.132
Async XLA Ops:
  6.3 55.2 %copy-start = (bf16[256,2048]{1,0:T(8,128)(2,1)S(1)}, bf16[256,2048]{1,0:T(8,128)(2,1)}, u32[]{:S(2)}) copy-start(bf16[256,2048]{1,0:T(8,128)(2,1)} %w_out_ref.1) | copy-start | bytes 3145732
  6.3 55.2 %copy-start.1 = (f32[64,384]{1,0:T(8,128)S(1)}, f32[64,384]{1,0:T(8,128)}, u32[]{:S(2)}) copy-start(f32[64,384]{1,0:T(8,128)} %get-tuple-element.14.next_ref) | copy-start | bytes 294916
